TPU v7x, 32 devices: a whole 2x2x4 slice. The times are simulated.
32 devices in a mesh: sp: 16 (over z, y, x), dp: 2 (over core).
Axes of the slice: x: 2, y: 2, z: 4, core: 2. Of those that a mesh axis runs over, the one named last changes fastest.
Arguments:
- glu_value: bfloat16 [2, 8192, 512], P('dp', 'sp'), may hold values from -6 to 6
- glu_gate: bfloat16 [2, 8192, 512], P('dp', 'sp'), may hold values from -8 to 8
- cotangent: bfloat16 [2, 8192, 2048], P('dp', 'sp'), may hold values from -8 to 8
- conv_weight: float32 [31, 512], replicated, may hold values from -1 to 1
- norm_gain: float32 [512], replicated, may hold values from 0.1 to 1.9
- norm_shift: float32 [512], replicated, may hold values from -3 to 3
- out_weight: bfloat16 [2048, 512], P('dp'), may hold values from -0.25 to 0.25
Outputs:
- grad_value: bfloat16 [2, 8192, 512], P('dp', 'sp')
- grad_gate: bfloat16 [2, 8192, 512], P('dp', 'sp')
- grad_out_weight: float32 [2048, 512], P('dp')
- grad_conv: float32 [31, 512], replicated
- grad_gain: float32 [512], replicated
- grad_shift: float32 [512], replicated
All inputs are finite; a program needn't handle non-finite values.
Results may differ from a plain program's by a relative error of at most 0.003.
Values may be sent and summed in bfloat16 or wider, within the bound.
No kernel may reach another device: no remote copies, remote signals or barrier semaphores. Data moves between devices by JAX's collectives and lax.ppermute only.
A program may use at most 64 MiB of HBM per device.

v0:
```python
import math

import jax
import jax.numpy as jnp
from jax import lax
from jax.sharding import PartitionSpec as P

epsilon = 1e-06


def from_behind(value, axis, by):
    count = lax.axis_size(axis)
    pairs = [(i, i + by) for i in range(count) if 0 <= i + by < count]
    return lax.ppermute(value, axis, pairs)


def per_device(glu_value, glu_gate, cotangent, conv_weight, norm_gain, norm_shift, out_weight):
    value_rows = glu_value[0]
    gate_rows = glu_gate[0]
    cotan_rows = cotangent[0]
    length = value_rows.shape[0]
    channels = value_rows.shape[1]
    tap_count = conv_weight.shape[0]
    halo_rows = tap_count - 1
    count_sp = lax.axis_size("sp")
    count_dp = lax.axis_size("dp")
    scale = 1.0 / math.sqrt(length * count_sp * count_dp)
    prior_value, prior_gate = from_behind(
        (value_rows[length - halo_rows :], gate_rows[length - halo_rows :]), "sp", 1
    )
    value_ext = jnp.concatenate([prior_value, value_rows], axis=0).astype(jnp.float32)
    gate_ext = jnp.concatenate([prior_gate, gate_rows], axis=0).astype(jnp.float32)
    gated_ext = value_ext * jax.nn.sigmoid(gate_ext)
    conv_rows = jnp.zeros((length, channels), jnp.float32)
    for offset in range(tap_count):
        conv_rows = conv_rows + conv_weight[offset] * gated_ext[offset : offset + length]
    centred = conv_rows - jnp.mean(conv_rows, axis=-1, keepdims=True)
    inv_std = lax.rsqrt(jnp.mean(centred * centred, axis=-1, keepdims=True) + epsilon)
    normed = centred * inv_std
    pre_act = normed * norm_gain + norm_shift
    sigmoid_pre = jax.nn.sigmoid(pre_act)
    act_rows = (pre_act * sigmoid_pre).astype(jnp.bfloat16)
    columns = cotan_rows
    grad_act = jnp.dot(
        columns,
        lax.all_gather(out_weight, "dp", axis=0, tiled=True),
        preferred_element_type=jnp.float32,
    )
    grad_pre = grad_act * sigmoid_pre * (1.0 + pre_act * (1.0 - sigmoid_pre))
    grad_normed = grad_pre * norm_gain
    grad_conv_rows = inv_std * (
        grad_normed
        - jnp.mean(grad_normed, axis=-1, keepdims=True)
        - normed * jnp.mean(grad_normed * normed, axis=-1, keepdims=True)
    )
    later_grads = from_behind(grad_conv_rows[:halo_rows], "sp", -1)
    padded_grad = jnp.concatenate([grad_conv_rows, later_grads], axis=0)
    grad_gated = jnp.zeros((length, channels), jnp.float32)
    for offset in range(tap_count):
        start = tap_count - 1 - offset
        grad_gated = grad_gated + conv_weight[offset] * padded_grad[start : start + length]
    grad_taps = jnp.stack(
        [
            jnp.sum(grad_conv_rows * gated_ext[offset : offset + length], axis=0)
            for offset in range(tap_count)
        ],
        axis=0,
    )
    sigmoid_gate = jax.nn.sigmoid(gate_ext[halo_rows:])
    grad_value = (grad_gated * sigmoid_gate).astype(jnp.bfloat16)
    grad_gate = (grad_gated * value_ext[halo_rows:] * sigmoid_gate * (1.0 - sigmoid_gate)).astype(
        jnp.bfloat16
    )
    grad_conv, grad_gain, grad_shift = lax.psum(
        (
            grad_taps * scale,
            jnp.sum(grad_pre * normed, axis=0) * scale,
            jnp.sum(grad_pre, axis=0) * scale,
        ),
        ("sp", "dp"),
    )
    columns = cotan_rows
    product = lax.dot_general(
        columns, act_rows, (((0,), (0,)), ((), ())), preferred_element_type=jnp.float32
    )
    partial_rows = lax.psum_scatter(product * scale, "dp", scatter_dimension=0, tiled=True)
    grad_out_weight = lax.psum(partial_rows, "sp")
    return (grad_value[None], grad_gate[None], grad_out_weight, grad_conv, grad_gain, grad_shift)


def solution(mesh):
    in_specs = (
        P("dp", "sp", None),
        P("dp", "sp", None),
        P("dp", "sp", None),
        P(),
        P(),
        P(),
        P("dp", None),
    )
    out_specs = (P("dp", "sp", None), P("dp", "sp", None), P("dp", None), P(), P(), P())
    return jax.shard_map(
        per_device, mesh=mesh, in_specs=in_specs, out_specs=out_specs, check_vma=False
    )
```

profile of v0, /device:TPU:0, one launch (start us, length us, event | category | flops | bytes accessed | tf_op | source)
XLA Modules:
  0.0 314.7 jit_solution(10922288983692130966)
XLA Ops:
  7.2 0.0 copy-start
  7.2 0.0 copy-start.5
  7.2 0.0 all-gather.2.cloned.1.call-start
  7.2 0.7 all-gather.2.cloned.1.call-update
  7.9 0.0 reduce-scatter.2.cloned.1.call-start
  8.0 0.8 slice_bitcast_fusion
  8.7 4.9 %collective-permute-start.1 = (bf16[30,512]{1,0:T(8,128)(2,1)S(1)}, bf16[30,512]{1,0:T(8,128)(2,1)S(1)}, u32[]{:S(2)}, u32[]{:S(2)}) collective-permute-start(bf16[30,512]{1,0:T(8,128)(2,1)S(1)} %slice_bitcast_fusion), channel_id=1, source_target_pairs={{0,2},{2,4},{4,6},{6,8},{8,10},{10,12},{12,14},{14,16},{16,18},{18... | collective-permute-start | bytes 92168 | tf_op jit(solution)/shard_map/ppermute | solution.py:14
  13.6 0.8 slice_bitcast_fusion.1
  14.4 3.4 %collective-permute-start = (bf16[30,512]{1,0:T(8,128)(2,1)S(1)}, bf16[30,512]{1,0:T(8,128)(2,1)S(1)}, u32[]{:S(2)}, u32[]{:S(2)}) collective-permute-start(bf16[30,512]{1,0:T(8,128)(2,1)S(1)} %slice_bitcast_fusion.1), channel_id=1, source_target_pairs={{0,2},{2,4},{4,6},{6,8},{8,10},{10,12},{12,14},{14,16},{16,18},{18... | collective-permute-start | bytes 92168 | tf_op jit(solution)/shard_map/ppermute | solution.py:14
  17.8 0.0 copy-done.5
  17.9 0.0 collective-permute-done.1
  17.9 1.5 collective-permute-done
  19.4 1.7 divide_multiply_fusion
  21.1 0.0 copy-start.6
  21.1 0.0 copy-start.7
  21.1 5.0 %fusion.113 = (f32[512]{0:T(512)S(1)}, f32[512,512]{1,0:T(8,128)S(1)}) fusion(f32[542,512]{1,0:T(8,128)S(1)} %divide_multiply_fusion, f32[512]{0:T(512)S(1)} %bitcast.148, f32[512]{0:T(512)S(1)} %bitcast.150, f32[512]{0:T(512)S(1)} %bitcast.92, f32[512]{0:T(512)S(1)} %bitcast.94, f32[512]{0:T(512)S(1)} %bitcast.96, f32[512]{0:T(512)S(1)} %bitcast.98, ...), kind=kLoop, calls=%fused_computation.212 | loop fusion | flops 16252416 | bytes 33619968 | tf_op jit(solution)/shard_map/reduce_sum | solution.py:37
  26.1 0.0 copy-start.2
  26.1 0.3 multiply_reduce_fusion.33
  26.4 0.7 copy-done.2
  27.0 0.0 copy-done
  27.0 0.0 copy-done.6
  27.1 3.4 %multiply_bitcast_fusion = f32[2048,512]{0,1:T(8,128)} fusion(bf16[1,512,2048]{2,1,0:T(8,128)(2,1)S(1)} %copy-done, f32[512,512]{1,0:T(8,128)S(1)} %get-tuple-element.54, f32[512]{0:T(512)S(1)} %copy-done.7, f32[512]{0:T(512)S(1)} %copy-done.6, f32[512]{0:T(512)S(1)} %add_rsqrt_fusion, f32[512]{0:T(512)S(1)} %broadcast_multiply_fusion.5), kind=kOutput, calls=%fused_computation.29 | convolution fusion | flops 1077149696 | bytes 7348224 | tf_op jit(solution)/shard_map/dot_general | solution.py:83
  30.5 0.0 reduce-scatter.2.cloned.1.call-update
  30.5 0.0 all-reduce.4.cloned.1.call-start
  30.5 0.0 copy-start.4
  30.5 2.4 maximum_convert_fusion.1
  32.9 1.2 maximum_convert_fusion
  34.1 5.1 %multiply_reduce_fusion = (f32[512]{0:T(512)}, f32[512]{0:T(512)S(1)}, f32[512]{0:T(512)S(1)}, f32[512]{0:T(512)}, f32[512,512]{1,0:T(8,128)}) fusion(f32[512,512]{1,0:T(8,128)} %copy-done.2, f32[512]{0:T(512)S(1)} %add_rsqrt_fusion, f32[512]{0:T(512)S(1)} %broadcast_multiply_fusion.5, f32[512]{0:T(512)S(1)} %copy-done.6, f32[512]{0:T(512)S(1)} %copy-done.7, ...), kind=kOutput, calls=%fused_computation.151 | convolution fusion | flops 1078720512 | bytes 6307840 | tf_op jit(solution)/shard_map/dot_general | solution.py:44
  39.2 5.3 %reduce-scatter.2.cloned.1.call-done = f32[1024,512]{0,1:T(8,128)} async-done(((f32[2048,512]{0,1:T(8,128)}), f32[1024,512]{0,1:T(8,128)}) %reduce-scatter.2.cloned.1.call-update) | async-done | bytes 2097168 | tf_op jit(solution)/shard_map/reduce_scatter | solution.py:86
  44.5 0.0 all-reduce.4.cloned.1.call-update
  44.5 0.0 all-reduce.6.cloned.1.call-start
  44.6 4.2 %multiply_reduce_fusion.1 = (f32[512]{0:T(512)S(1)}, f32[512]{0:T(512)S(1)}, f32[512]{0:T(512)S(1)}, f32[512]{0:T(512)S(1)}, f32[512]{0:T(512)S(1)}, /*index=5*/...) fusion(f32[542,512]{1,0:T(8,128)S(1)} %divide_multiply_fusion, ...), kind=kLoop, calls=%fused_computation.152 | loop fusion | flops 11262976 | bytes 22067200 | tf_op jit(solution)/shard_map/reduce_sum | solution.py:64
  48.8 1.5 collective-permute-start.2
  50.3 2.3 multiply_reduce_fusion.19
  52.6 1.6 stack.127
  54.2 0.6 broadcast_multiply_fusion
  54.8 1.3 broadcast_multiply_fusion.1
  56.1 0.0 all-reduce.6.cloned.1.call-update
  56.1 0.0 copy-start.3
  56.1 0.0 collective-permute-done.2
  56.1 23.0 %fusion.105 = (bf16[1,512,512]{2,1,0:T(8,128)(2,1)}, f32[512,512]{1,0:T(8,128)S(1)}) fusion(f32[542,512]{1,0:T(8,128)} %maximum_convert_fusion, f32[542,512]{1,0:T(8,128)} %maximum_convert_fusion.1, f32[512,512]{1,0:T(8,128)} %copy-done.1, f32[512]{0:T(512)S(1)} %bitcast.149, f32[30,512]{1,0:T(8,128)S(1)} %collective-permute-done.2, f32[512]{0:T(512)S(1)} %bitcast.151, ...), kind=kLoop, calls=%fused_computation.196 | loop fusion | flops 25952256 | bytes 4843520 | tf_op jit(solution)/shard_map/broadcast_in_dim | solution.py:88
  79.2 1.1 fusion.104
  80.2 97.6 %all-reduce.4.cloned.1.call-done = f32[1024,512]{0,1:T(8,128)} async-done(((f32[1024,512]{0,1:T(8,128)}), f32[1024,512]{0,1:T(8,128)}) %all-reduce.4.cloned.1.call-update) | async-done | bytes 2097168 | tf_op jit(solution)/shard_map/psum | solution.py:87
  177.9 2.9 copy.13
  180.7 123.4 %all-reduce.6.cloned.1.call-done = (f32[31,512]{1,0:T(8,128)}, f32[512]{0:T(512)}, f32[512]{0:T(512)}) async-done(((f32[31,512]{1,0:T(8,128)}, f32[512]{0:T(512)}, f32[512]{0:T(512)}), (f32[31,512]{1,0:T(8,128)}, f32[512]{0:T(512)}, f32[512]{0:T(512)})) %all-reduce.6.cloned.1.call-update) | async-done | bytes 67600 | tf_op jit(solution)/shard_map/psum | solution.py:74
  304.2 1.5 copy.18
  305.6 1.3 copy.19
  306.9 1.2 copy.20
  (12 shorter events, 0.1 us)
Async XLA Ops:
  7.2 19.9 %copy-start = (bf16[1,512,2048]{2,1,0:T(8,128)(2,1)S(1)}, bf16[1,512,2048]{2,1,0:T(8,128)(2,1)}, u32[]{:S(2)}) copy-start(bf16[1,512,2048]{2,1,0:T(8,128)(2,1)} %param.9) | copy-start | bytes 6291460
  7.2 10.6 %copy-start.5 = (f32[31,512]{1,0:T(8,128)S(1)}, f32[31,512]{1,0:T(8,128)}, u32[]{:S(2)}) copy-start(f32[31,512]{1,0:T(8,128)} %param.10) | copy-start | bytes 190468
  7.2 26.9 %all-gather.2.cloned.1.call-start = ((), (), s32[]{:S(2)}) async-start(), calls=%async_computation.1 | async-start | bytes 3145728 | tf_op jit(solution)/shard_map/all_gather | solution.py:46
  7.9 36.6 %reduce-scatter.2.cloned.1.call-start = ((), (), s32[]{:S(2)}) async-start(), calls=%async_computation.2 | async-start | bytes 6291456 | tf_op jit(solution)/shard_map/reduce_scatter | solution.py:86
  8.7 9.1 %collective-permute-start.1 = (bf16[30,512]{1,0:T(8,128)(2,1)S(1)}, bf16[30,512]{1,0:T(8,128)(2,1)S(1)}, u32[]{:S(2)}, u32[]{:S(2)}) collective-permute-start(bf16[30,512]{1,0:T(8,128)(2,1)S(1)} %slice_bitcast_fusion), channel_id=1, source_target_pairs={{0,2},{2,4},{4,6},{6,8},{8,10},{10,12},{12,14},{14,16},{16,18},{18... | collective-permute-start | bytes 92168 | tf_op jit(solution)/shard_map/ppermute | solution.py:14
  14.4 5.0 %collective-permute-start = (bf16[30,512]{1,0:T(8,128)(2,1)S(1)}, bf16[30,512]{1,0:T(8,128)(2,1)S(1)}, u32[]{:S(2)}, u32[]{:S(2)}) collective-permute-start(bf16[30,512]{1,0:T(8,128)(2,1)S(1)} %slice_bitcast_fusion.1), channel_id=1, source_target_pairs={{0,2},{2,4},{4,6},{6,8},{8,10},{10,12},{12,14},{14,16},{16,18},{18... | collective-permute-start | bytes 92168 | tf_op jit(solution)/shard_map/ppermute | solution.py:14
  21.1 6.0 %copy-start.6 = (f32[512]{0:T(512)S(1)}, f32[512]{0:T(512)}, u32[]{:S(2)}) copy-start(f32[512]{0:T(512)} %param.11) | copy-start | bytes 6148
  21.1 6.0 %copy-start.7 = (f32[512]{0:T(512)S(1)}, f32[512]{0:T(512)}, u32[]{:S(2)}) copy-start(f32[512]{0:T(512)} %param.12) | copy-start | bytes 6148
  26.1 1.0 copy-start.2
  30.5 147.4 %all-reduce.4.cloned.1.call-start = ((), (), s32[]{:S(2)}) async-start(), calls=%async_computation.3 | async-start | bytes 4194304 | tf_op jit(solution)/shard_map/psum | solution.py:87
  30.5 2.4 copy-start.4
  44.5 259.6 %all-reduce.6.cloned.1.call-start = ((), (), s32[]{:S(2)}) async-start(), calls=%async_computation.4 | async-start | bytes 139264 | tf_op jit(solution)/shard_map/psum | solution.py:74
  48.8 3.8 %copy-start.1 = (f32[512,512]{1,0:T(8,128)}, f32[512,512]{1,0:T(8,128)S(1)}, u32[]{:S(2)}) copy-start(f32[512,512]{1,0:T(8,128)S(1)} %get-tuple-element.50) | copy-start | bytes 3145732
  48.8 7.3 %collective-permute-start.2 = (f32[30,512]{1,0:T(8,128)S(1)}, f32[30,512]{1,0:T(8,128)S(1)}, u32[]{:S(2)}, u32[]{:S(2)}) collective-permute-start(f32[30,512]{1,0:T(8,128)S(1)} %slice.489), channel_id=1, source_target_pairs={{2,0},{4,2},{6,4},{8,6},{10,8},{12,10},{14,12},{16,14},{18,16},{20... | collective-permute-start | bytes 184328 | tf_op jit(solution)/shard_map/ppermute | solution.py:14
  56.1 23.1 %copy-start.3 = (f32[542,512]{1,0:T(8,128)S(1)}, f32[542,512]{1,0:T(8,128)}, u32[]{:S(2)}) copy-start(f32[542,512]{1,0:T(8,128)} %maximum_convert_fusion.1) | copy-start | bytes 3330052
Sparse Core Ops, SparseCore 0:
  9.5 13.2 all-gather.1
  30.6 13.8 reduce-scatter.1
  50.0 127.8 all-reduce.3
  184.2 119.8 all-reduce.5
where the time goes:
time: 317 us; the launch traced here: 315 us
  waiting for transfers between devices  229 us (72%)
  other arithmetic  43 us (14%)
  between operations  14 us (4%)
  local copies, waits for them, and re-layouts  10.7 us (3%)
  starting transfers between devices  9.9 us (3%)
  matrix products  8.5 us (3%)
    psum x1, waiting for transfers between devices, per_device(): lax.psum((grad_taps * scale, jnp.sum(grad_pre * normed, axis=0) * scale,...  123 us
    psum x1, waiting for transfers between devices, per_device(): grad_out_weight = lax.psum(partial_rows, 'sp')  97.6 us
    broadcast_in_dim x1, other arithmetic, per_device(): grad_gate[None]  23 us
    ppermute x3, starting transfers between devices, from_behind(): return lax.ppermute(value, axis, pairs)  9.74 us
    unnamed x20, local copies, waits for them, and re-layouts  7.56 us
    reduce_sum x2, other arithmetic, per_device(): jnp.sum(grad_conv_rows * gated_ext[offset:offset + length], axis=0)  6.52 us
  transfers between devices with their start and end apart: 7, of which 4 were waited for; matrix products, arithmetic and copies ran while one was open for 18% of the time, Pallas kernels for 0%

commit v1 on v0

--- a/solution.py
+++ b/solution.py
@@ -12,6 +12,74 @@
     count = lax.axis_size(axis)
     pairs = [(i, i + by) for i in range(count) if 0 <= i + by < count]
     return lax.ppermute(value, axis, pairs)
+
+
+def exchange(value, axis, offset):
+    count = lax.axis_size(axis)
+    return lax.ppermute(value, axis, [(i, i ^ offset) for i in range(count)])
+
+
+def levels_of(count):
+    bits = count.bit_length() - 1
+    return [(1 << low, 1 << min(2, bits - low)) for low in range(0, bits, 2)]
+
+
+def digit(level):
+    low, width = level
+    return (lax.axis_index("sp") // low) % width
+
+
+def reduce_level(total, level):
+    low, width = level
+    mine = digit(level)
+    parts = total.reshape((width, total.shape[0] // width) + total.shape[1:])
+    arrived = [
+        exchange(
+            lax.dynamic_index_in_dim(parts, mine ^ other, 0, False).astype(jnp.bfloat16),
+            "sp",
+            other * low,
+        )
+        for other in range(width - 1, 0, -1)
+    ]
+    kept = lax.dynamic_index_in_dim(parts, mine, 0, False)
+    for part in arrived:
+        kept = kept + part.astype(jnp.float32)
+    return kept
+
+
+def gather_level(rows, level):
+    low, width = level
+    mine = digit(level)
+    pieces = [rows] + [None] * (width - 1)
+    for other in range(width - 1, 0, -1):
+        pieces[other] = exchange(rows, "sp", other * low)
+    half = 1
+    while half < width:
+        swap = (mine // half) % 2 == 1
+        paired = []
+        for i in range(0, len(pieces), 2):
+            first, second = pieces[i], pieces[i + 1]
+            paired.append(
+                jnp.where(
+                    swap,
+                    jnp.concatenate([second, first], axis=0),
+                    jnp.concatenate([first, second], axis=0),
+                )
+            )
+        pieces = paired
+        half *= 2
+    return pieces[0]
+
+
+def tree(items):
+    while len(items) > 1:
+        items = [items[i] + items[i + 1] for i in range(0, len(items), 2)]
+    return items[0]
+
+
+def all_sum(value, axis, level):
+    low, width = level
+    return tree([value] + [exchange(value, axis, other * low) for other in range(1, width)])
 
 
 def per_device(glu_value, glu_gate, cotangent, conv_weight, norm_gain, norm_shift, out_weight):
@@ -71,20 +139,36 @@
     grad_gate = (grad_gated * value_ext[halo_rows:] * sigmoid_gate * (1.0 - sigmoid_gate)).astype(
         jnp.bfloat16
     )
-    grad_conv, grad_gain, grad_shift = lax.psum(
-        (
-            grad_taps * scale,
-            jnp.sum(grad_pre * normed, axis=0) * scale,
-            jnp.sum(grad_pre, axis=0) * scale,
-        ),
-        ("sp", "dp"),
+    levels = levels_of(count_sp)
+    product = lax.dot_general(
+        cotan_rows, act_rows, (((0,), (0,)), ((), ())), preferred_element_type=jnp.float32
     )
-    columns = cotan_rows
-    product = lax.dot_general(
-        columns, act_rows, (((0,), (0,)), ((), ())), preferred_element_type=jnp.float32
-    )
-    partial_rows = lax.psum_scatter(product * scale, "dp", scatter_dimension=0, tiled=True)
-    grad_out_weight = lax.psum(partial_rows, "sp")
+    features = product.shape[0] // count_dp
+    blocks = (product * scale).reshape(count_dp, features, channels)
+    index_dp = lax.axis_index("dp")
+    arrived = [
+        exchange(lax.dynamic_index_in_dim(blocks, index_dp ^ other, 0, False), "dp", other)
+        for other in range(1, count_dp)
+    ]
+    total = tree([lax.dynamic_index_in_dim(blocks, index_dp, 0, False)] + arrived)
+    cut = 3 * features // 4
+    if len(levels) > 1 and cut % (16 * count_sp) == 0 and (features - cut) % (16 * count_sp) == 0:
+        colours = [(total[:cut], levels), (total[cut:], levels[1:] + levels[:1])]
+    else:
+        colours = [(total, levels)]
+    states = [c[0] for c in colours]
+    for step in range(len(levels)):
+        states = [reduce_level(v, order[step]) for v, (_, order) in zip(states, colours)]
+    states = [v.astype(jnp.bfloat16) for v in states]
+    small = jnp.concatenate(
+        [grad_taps, jnp.sum(grad_pre * normed, axis=0)[None], jnp.sum(grad_pre, axis=0)[None]]
+    ) * scale
+    small = all_sum(small, "dp", (1, count_dp))
+    for step in reversed(range(len(levels))):
+        states = [gather_level(v, order[step]) for v, (_, order) in zip(states, colours)]
+        small = all_sum(small, "sp", levels[len(levels) - 1 - step])
+    grad_out_weight = jnp.concatenate(states, axis=0).astype(jnp.float32)
+    grad_conv, grad_gain, grad_shift = small[:tap_count], small[tap_count], small[tap_count + 1]
     return (grad_value[None], grad_gate[None], grad_out_weight, grad_conv, grad_gain, grad_shift)
 
 

time: 317 us -> 145 us (0.46)
  waiting for transfers between devices: 229 us -> 18.4 us
  starting transfers between devices: 9.9 us -> 58.4 us
  other arithmetic: 43 us -> 27.3 us
  local copies, waits for them, and re-layouts: 10.7 us -> 17.4 us
    psum x2 -> x0, waiting for transfers between devices: 221 us -> none  [the longest x1 123 us: per_device(): lax.psum((grad_taps * scale, jnp.sum(grad_pre * normed, axis=0) * scale,...]
    ppermute x0 -> x32, starting transfers between devices: none -> 48.6 us  [exchange(): return lax.ppermute(value, axis, [(i, i ^ offset) for i in range(count)])]
    ppermute x0 -> x32, waiting for transfers between devices: none -> 17.7 us  [exchange(): return lax.ppermute(value, axis, [(i, i ^ offset) for i in range(count)])]
    broadcast_in_dim x1, other arithmetic: 23 us -> 6.09 us  [per_device(): grad_gate[None]]
    unnamed x20 -> x22, local copies, waits for them, and re-layouts: 7.56 us -> 0.75 us
    reshape x0 -> x1, local copies, waits for them, and re-layouts: none -> 5.35 us  [per_device(): blocks = (product * scale).reshape(count_dp, features, channels)]
    reduce_scatter x1 -> x0, waiting for transfers between devices: 5.34 us -> none  [per_device(): lax.psum_scatter(product * scale, 'dp', scatter_dimension=0, tiled=True)]
  transfers between devices with their start and end apart: 7 -> 36, of which waited for: 4 -> 14; matrix products, arithmetic and copies ran while one was open for 18% -> 34% of each run, Pallas kernels for 0% -> 0%
where the time goes in v1:
time: 145 us; the launch traced here: 144 us
  starting transfers between devices  58.4 us (40%)
  other arithmetic  27.3 us (19%)
  waiting for transfers between devices  18.4 us (13%)
  local copies, waits for them, and re-layouts  17.4 us (12%)
  between operations  14.6 us (10%)
  matrix products  7.77 us (5%)
    ppermute x32, starting transfers between devices, exchange(): return lax.ppermute(value, axis, [(i, i ^ offset) for i in range(count)])  48.6 us
    ppermute x32, waiting for transfers between devices, exchange(): return lax.ppermute(value, axis, [(i, i ^ offset) for i in range(count)])  17.7 us
    ppermute x3, starting transfers between devices, from_behind(): return lax.ppermute(value, axis, pairs)  9.74 us
    broadcast_in_dim x1, other arithmetic, per_device(): grad_gate[None]  6.09 us
    reduce_sum x2, other arithmetic, per_device(): jnp.sum(grad_conv_rows * gated_ext[offset:offset + length], axis=0)  5.52 us
    reshape x1, local copies, waits for them, and re-layouts, per_device(): blocks = (product * scale).reshape(count_dp, features, channels)  5.35 us
    reduce_sum x1, other arithmetic, per_device(): centred = conv_rows - jnp.mean(conv_rows, axis=-1, keepdims=True)  4.98 us
    dot_general x1, matrix products, per_device(): jnp.dot(columns, lax.all_gather(out_weight, 'dp', axis=0, tiled=True), pr...  4.33 us
  transfers between devices with their start and end apart: 36, of which 14 were waited for; matrix products, arithmetic and copies ran while one was open for 34% of the time, Pallas kernels for 0%

profile of v1, /device:TPU:0, one launch (start us, length us, event | category | flops | bytes accessed | tf_op | source)
XLA Modules:
  0.0 143.9 jit_solution(9001352563949752344)
XLA Ops:
  8.7 4.9 %collective-permute-start.1 = (bf16[30,512]{1,0:T(8,128)(2,1)S(1)}, bf16[30,512]{1,0:T(8,128)(2,1)S(1)}, u32[]{:S(2)}, u32[]{:S(2)}) collective-permute-start(bf16[30,512]{1,0:T(8,128)(2,1)S(1)} %slice_bitcast_fusion), channel_id=1, source_target_pairs={{0,2},{2,4},{4,6},{6,8},{8,10},{10,12},{12,14},{14,16},{16,18},{18... | collective-permute-start | bytes 92168 | tf_op jit(solution)/shard_map/ppermute | solution.py:14
  14.3 3.4 %collective-permute-start = (bf16[30,512]{1,0:T(8,128)(2,1)S(1)}, bf16[30,512]{1,0:T(8,128)(2,1)S(1)}, u32[]{:S(2)}, u32[]{:S(2)}) collective-permute-start(bf16[30,512]{1,0:T(8,128)(2,1)S(1)} %slice_bitcast_fusion.1), channel_id=1, source_target_pairs={{0,2},{2,4},{4,6},{6,8},{8,10},{10,12},{12,14},{14,16},{16,18},{18... | collective-permute-start | bytes 92168 | tf_op jit(solution)/shard_map/ppermute | solution.py:14
  17.8 1.2 fusion.138
  20.1 1.6 %divide_multiply_fusion = f32[542,512]{1,0:T(8,128)S(1)} fusion(bf16[512,512]{1,0:T(8,128)(2,1)} %bitcast.155, bf16[30,512]{1,0:T(8,128)(2,1)S(1)} %collective-permute-done.1, bf16[512,512]{1,0:T(8,128)(2,1)} %bitcast.157, bf16[30,512]{1,0:T(8,128)(2,1)S(1)} %collective-permute-done), kind=kLoop, calls=%fused_computation.37 | loop fusion | flops 3330048 | bytes 2220032 | tf_op jit(solution)/shard_map/mul | solution.py:101
  21.8 5.0 %fusion.136 = (f32[512]{0:T(512)S(1)}, f32[512,512]{1,0:T(8,128)S(1)}) fusion(f32[542,512]{1,0:T(8,128)S(1)} %divide_multiply_fusion, f32[512]{0:T(512)S(1)} %bitcast.223, f32[512]{0:T(512)S(1)} %bitcast.225, f32[512]{0:T(512)S(1)} %bitcast.167, f32[512]{0:T(512)S(1)} %bitcast.169, f32[512]{0:T(512)S(1)} %bitcast.171, f32[512]{0:T(512)S(1)} %bitcast.173, ...), kind=kLoop, calls=%fused_computation.266 | loop fusion | flops 16252416 | bytes 33619968 | tf_op jit(solution)/shard_map/reduce_sum | solution.py:105
  27.8 3.4 %multiply_bitcast_fusion = f32[2048,512]{0,1:T(8,128)} fusion(bf16[1,512,2048]{2,1,0:T(8,128)(2,1)S(1)} %copy-done, f32[512,512]{1,0:T(8,128)S(1)} %get-tuple-element.45, f32[512]{0:T(512)S(1)} %copy-done.10, f32[512]{0:T(512)S(1)} %copy-done.9, f32[512]{0:T(512)S(1)} %add_rsqrt_fusion, f32[512]{0:T(512)S(1)} %broadcast_multiply_fusion.3), kind=kOutput, calls=%fused_computation.29 | convolution fusion | flops 1077149696 | bytes 7348224 | tf_op jit(solution)/shard_map/dot_general | solution.py:143
  31.2 5.3 %copy.15 = f32[2048,512]{1,0:T(8,128)} copy(f32[2048,512]{0,1:T(8,128)} %multiply_bitcast_fusion) | data formatting | bytes 8388608 | tf_op jit(solution)/shard_map/reshape | solution.py:147
  36.6 3.1 %dynamic-slice_bitcast_fusion = f32[1024,512]{1,0:T(8,128)} fusion(f32[2,1024,512]{2,1,0:T(8,128)} %bitcast.151, s32[]{:T(128)S(6)} %select_n.207), kind=kLoop, calls=%fused_computation.34 | loop fusion | bytes 4194308 | tf_op jit(solution)/shard_map/jit(dynamic_index_in_dim)/squeeze | solution.py:150
  39.7 1.2 maximum_convert_fusion.2
  40.9 1.2 maximum_convert_fusion.1
  42.1 4.3 %multiply_reduce_fusion = (f32[512]{0:T(512)}, f32[512]{0:T(512)S(1)}, f32[512]{0:T(512)S(1)}, f32[512]{0:T(512)}, f32[512,512]{1,0:T(8,128)S(1)}) fusion(f32[512,512]{1,0:T(8,128)} %copy-done.3, f32[512]{0:T(512)S(1)} %add_rsqrt_fusion, f32[512]{0:T(512)S(1)} %broadcast_multiply_fusion.3, f32[512]{0:T(512)S(1)} %copy-done.9, f32[512]{0:T(512)S(1)} %copy-done.10, ...), kind=kOutput, calls=%fused_computation.154 | convolution fusion | flops 1078720512 | bytes 6307840 | tf_op jit(solution)/shard_map/dot_general | solution.py:112
  46.4 3.2 %multiply_reduce_fusion.1 = (f32[512]{0:T(512)S(1)}, f32[512]{0:T(512)S(1)}, f32[512]{0:T(512)S(1)}, f32[512]{0:T(512)S(1)}, f32[512]{0:T(512)S(1)}, /*index=5*/...) fusion(f32[542,512]{1,0:T(8,128)S(1)} %divide_multiply_fusion, ...), kind=kLoop, calls=%fused_computation.155 | loop fusion | flops 11262976 | bytes 22067200 | tf_op jit(solution)/shard_map/reduce_sum | solution.py:132
  49.7 1.5 %collective-permute-start.2 = (f32[30,512]{1,0:T(8,128)S(1)}, f32[30,512]{1,0:T(8,128)S(1)}, u32[]{:S(2)}, u32[]{:S(2)}) collective-permute-start(f32[30,512]{1,0:T(8,128)S(1)} %slice.509), channel_id=1, source_target_pairs={{2,0},{4,2},{6,4},{8,6},{10,8},{12,10},{14,12},{16,14},{18,16},{20... | collective-permute-start | bytes 184328 | tf_op jit(solution)/shard_map/ppermute | solution.py:14
  51.1 2.3 %multiply_reduce_fusion.19 = (f32[512]{0:T(512)S(1)}, f32[512]{0:T(512)S(1)}, f32[512]{0:T(512)S(1)}, f32[512]{0:T(512)}, f32[512]{0:T(512)}, /*index=5*/f32[512...) fusion(f32[512,512]{1,0:T(8,128)S(1)} %get-tuple-element.41, ...), kind=kLoop, calls=%fused_computation.173 | loop fusion | flops 6809088 | bytes 14706688 | tf_op jit(solution)/shard_map/reduce_sum | solution.py:132
  53.5 2.9 %concatenate.115 = f32[33,512]{1,0:T(8,128)S(1)} concatenate(f32[1,512]{1,0:T(1,128)} %bitcast.257, f32[1,512]{1,0:T(1,128)} %bitcast.256, f32[1,512]{1,0:T(1,128)} %bitcast.255, f32[1,512]{1,0:T(1,128)} %bitcast.254, f32[1,512]{1,0:T(1,128)} %bitcast.253, f32[1,512]{1,0:T(1,128)} %bitcast.252, f32[1,512]{1,0:T(1,128)} %bitcast.251, f32[1,512]{1,0:T(1,128)} %bitcast.250, ...), dimensions={0} | concatenate | bytes 135168 | tf_op jit(solution)/shard_map/concatenate | solution.py:163
  57.0 2.7 %bitcast_add_fusion = f32[1024,512]{1,0:T(8,128)S(1)} fusion(f32[1024,512]{1,0:T(8,128)} %collective-permute-done.3, f32[2,1024,512]{2,1,0:T(8,128)} %bitcast.152, s32[]{:T(128)S(6)} %select_n.206), kind=kLoop, calls=%fused_computation.30 | loop fusion | flops 524288 | bytes 6291460 | tf_op jit(solution)/shard_map/add | solution.py:76
  59.9 6.4 %collective-permute-start.16 = (bf16[64,512]{1,0:T(8,128)(2,1)S(1)}, bf16[64,512]{1,0:T(8,128)(2,1)S(1)}, u32[]{:S(2)}, u32[]{:S(2)}) collective-permute-start(bf16[64,512]{1,0:T(8,128)(2,1)S(1)} %get-tuple-element.49), channel_id=1, source_target_pairs={{0,24},{2,26},{4,28},{6,30},{8,16},{10,18},{12,20},{14,22},{16,8},... | collective-permute-start | bytes 196616 | tf_op jit(solution)/shard_map/ppermute | solution.py:19
  67.0 1.8 %collective-permute-start.4 = (bf16[192,512]{1,0:T(8,128)(2,1)S(1)}, bf16[192,512]{1,0:T(8,128)(2,1)S(1)}, u32[]{:S(2)}, u32[]{:S(2)}) collective-permute-start(bf16[192,512]{1,0:T(8,128)(2,1)S(1)} %get-tuple-element.46), channel_id=1, source_target_pairs={{0,6},{2,4},{4,2},{6,0},{8,14},{10,12},{12,10},{14,8},{16,22},{18,... | collective-permute-start | bytes 589832 | tf_op jit(solution)/shard_map/ppermute | solution.py:19
  68.8 6.1 %fusion.105 = (bf16[1,512,512]{2,1,0:T(8,128)(2,1)}, f32[512,512]{1,0:T(8,128)S(1)}) fusion(f32[542,512]{1,0:T(8,128)S(1)} %copy-done.6, f32[542,512]{1,0:T(8,128)S(1)} %copy-done.5, f32[512,512]{1,0:T(8,128)S(1)} %copy-done.2, f32[512]{0:T(512)S(1)} %bitcast.224, f32[30,512]{1,0:T(8,128)S(1)} %collective-permute-done.2, f32[512]{0:T(512)S(1)} %bitcast.226, ...), kind=kLoop, calls=%fused_computation.200 | loop fusion | flops 25952256 | bytes 4843520 | tf_op jit(solution)/shard_map/broadcast_in_dim | solution.py:172
  75.0 1.3 collective-permute-start.19
  76.2 1.5 %collective-permute-start.21 = (bf16[16,512]{1,0:T(8,128)(2,1)S(1)}, bf16[16,512]{1,0:T(8,128)(2,1)S(1)}, u32[]{:S(2)}, u32[]{:S(2)}) collective-permute-start(bf16[16,512]{1,0:T(8,128)(2,1)S(1)} %get-tuple-element.56), channel_id=1, source_target_pairs={{0,2},{2,0},{4,6},{6,4},{8,10},{10,8},{12,14},{14,12},{16,18},{18,... | collective-permute-start | bytes 49160 | tf_op jit(solution)/shard_map/ppermute | solution.py:19
  78.5 1.1 fusion.104
  80.3 1.2 collective-permute-done.20
  82.1 1.8 %collective-permute-start.31 = (f32[33,512]{1,0:T(8,128)S(1)}, f32[33,512]{1,0:T(8,128)S(1)}, u32[]{:S(2)}, u32[]{:S(2)}) collective-permute-start(f32[33,512]{1,0:T(8,128)S(1)} %fusion.134), channel_id=1, source_target_pairs={{0,6},{2,4},{4,2},{6,0},{8,14},{10,12},{12,10},{14,8},{16,22},{18,... | collective-permute-start | bytes 202760 | tf_op jit(solution)/shard_map/ppermute | solution.py:19
  83.9 1.2 collective-permute-start.23
  85.1 1.3 collective-permute-done.24
  86.4 1.4 collective-permute-start.22
  89.2 2.0 %collective-permute-done.22 = bf16[16,512]{1,0:T(8,128)(2,1)S(1)} collective-permute-done((bf16[16,512]{1,0:T(8,128)(2,1)S(1)}, bf16[16,512]{1,0:T(8,128)(2,1)S(1)}, u32[]{:S(2)}, u32[]{:S(2)}) %collective-permute-start.22) | collective-permute-done | bytes 16416 | tf_op jit(solution)/shard_map/ppermute | solution.py:19
  91.9 1.3 collective-permute-start.5
  93.2 1.4 collective-permute-start.27
  94.6 1.0 collective-permute-done.29
  95.6 2.3 %collective-permute-start.26 = (bf16[64,512]{1,0:T(8,128)(2,1)S(1)}, bf16[64,512]{1,0:T(8,128)(2,1)S(1)}, u32[]{:S(2)}, u32[]{:S(2)}) collective-permute-start(bf16[64,512]{1,0:T(8,128)(2,1)S(1)} %maximum_select_fusion.9), channel_id=1, source_target_pairs={{0,16},{2,18},{4,20},{6,22},{8,24},{10,26},{12,28},{14,30},{16,0},... | collective-permute-start | bytes 196616 | tf_op jit(solution)/shard_map/ppermute | solution.py:19
  97.9 3.3 %collective-permute-start.25 = (bf16[64,512]{1,0:T(8,128)(2,1)S(1)}, bf16[64,512]{1,0:T(8,128)(2,1)S(1)}, u32[]{:S(2)}, u32[]{:S(2)}) collective-permute-start(bf16[64,512]{1,0:T(8,128)(2,1)S(1)} %maximum_select_fusion.9), channel_id=1, source_target_pairs={{0,24},{2,26},{4,28},{6,30},{8,16},{10,18},{12,20},{14,22},{16,8},... | collective-permute-start | bytes 196616 | tf_op jit(solution)/shard_map/ppermute | solution.py:19
  101.2 6.6 %collective-permute-start.34 = (f32[33,512]{1,0:T(8,128)S(1)}, f32[33,512]{1,0:T(8,128)S(1)}, u32[]{:S(2)}, u32[]{:S(2)}) collective-permute-start(f32[33,512]{1,0:T(8,128)S(1)} %add_add_fusion.1), channel_id=1, source_target_pairs={{0,24},{2,26},{4,28},{6,30},{8,16},{10,18},{12,20},{14,22},{16,8},... | collective-permute-start | bytes 202760 | tf_op jit(solution)/shard_map/ppermute | solution.py:19
  109.1 2.5 %collective-permute-start.9 = (bf16[48,512]{1,0:T(8,128)(2,1)S(1)}, bf16[48,512]{1,0:T(8,128)(2,1)S(1)}, u32[]{:S(2)}, u32[]{:S(2)}) collective-permute-start(bf16[48,512]{1,0:T(8,128)(2,1)S(1)} %get-tuple-element.53), channel_id=1, source_target_pairs={{0,8},{2,10},{4,12},{6,14},{8,0},{10,2},{12,4},{14,6},{16,24},{18,... | collective-permute-start | bytes 147464 | tf_op jit(solution)/shard_map/ppermute | solution.py:19
  111.6 1.4 collective-permute-start.8
  113.1 1.4 collective-permute-done.7
  114.5 1.4 collective-permute-start.32
  115.9 1.5 %collective-permute-done.8 = bf16[48,512]{1,0:T(8,128)(2,1)S(1)} collective-permute-done((bf16[48,512]{1,0:T(8,128)(2,1)S(1)}, bf16[48,512]{1,0:T(8,128)(2,1)S(1)}, u32[]{:S(2)}, u32[]{:S(2)}) %collective-permute-start.8) | collective-permute-done | bytes 49184 | tf_op jit(solution)/shard_map/ppermute | solution.py:19
  117.5 1.4 collective-permute-done.32
  119.0 1.2 collective-permute-start.11
  120.2 2.6 %collective-permute-start.10 = (bf16[48,512]{1,0:T(8,128)(2,1)S(1)}, bf16[48,512]{1,0:T(8,128)(2,1)S(1)}, u32[]{:S(2)}, u32[]{:S(2)}) collective-permute-start(bf16[48,512]{1,0:T(8,128)(2,1)S(1)} %fusion.120), channel_id=1, source_target_pairs={{0,24},{2,26},{4,28},{6,30},{8,16},{10,18},{12,20},{14,22},{16,8},... | collective-permute-start | bytes 147464 | tf_op jit(solution)/shard_map/ppermute | solution.py:19
  122.9 1.2 collective-permute-done.11
  124.1 2.0 %collective-permute-done.10 = bf16[48,512]{1,0:T(8,128)(2,1)S(1)} collective-permute-done((bf16[48,512]{1,0:T(8,128)(2,1)S(1)}, bf16[48,512]{1,0:T(8,128)(2,1)S(1)}, u32[]{:S(2)}, u32[]{:S(2)}) %collective-permute-start.10) | collective-permute-done | bytes 49184 | tf_op jit(solution)/shard_map/ppermute | solution.py:19
  127.2 1.1 collective-permute-start.14
  128.2 1.5 %collective-permute-start.13 = (bf16[192,512]{1,0:T(8,128)(2,1)S(1)}, bf16[192,512]{1,0:T(8,128)(2,1)S(1)}, u32[]{:S(2)}, u32[]{:S(2)}) collective-permute-start(bf16[192,512]{1,0:T(8,128)(2,1)S(1)} %maximum_select_fusion.4), channel_id=1, source_target_pairs={{0,6},{2,4},{4,2},{6,0},{8,14},{10,12},{12,10},{14,8},{16,22},{18,... | collective-permute-start | bytes 589832 | tf_op jit(solution)/shard_map/ppermute | solution.py:19
  132.8 2.2 %collective-permute-done.13 = bf16[192,512]{1,0:T(8,128)(2,1)S(1)} collective-permute-done((bf16[192,512]{1,0:T(8,128)(2,1)S(1)}, bf16[192,512]{1,0:T(8,128)(2,1)S(1)}, u32[]{:S(2)}, u32[]{:S(2)}) %collective-permute-start.13) | collective-permute-done | bytes 196640 | tf_op jit(solution)/shard_map/ppermute | solution.py:19
  135.5 1.6 %maximum_convert_fusion = f32[1024,512]{1,0:T(8,128)} fusion(bf16[256,512]{1,0:T(8,128)(2,1)S(1)} %maximum_select_fusion.3, bf16[768,512]{1,0:T(8,128)(2,1)S(1)} %maximum_select_fusion), kind=kLoop, calls=%fused_computation.153 | loop fusion | flops 2097152 | bytes 3145728 | tf_op jit(solution)/shard_map/convert_element_type | solution.py:170
  (99 shorter events, 16.1 us)
Async XLA Ops:
  7.2 20.6 %copy-start = (bf16[1,512,2048]{2,1,0:T(8,128)(2,1)S(1)}, bf16[1,512,2048]{2,1,0:T(8,128)(2,1)}, u32[]{:S(2)}) copy-start(bf16[1,512,2048]{2,1,0:T(8,128)(2,1)} %param.9) | copy-start | bytes 6291460
  7.2 34.9 %all-gather.2.cloned.1.call-start = ((), (), s32[]{:S(2)}) async-start(), calls=%async_computation | async-start | bytes 3145728 | tf_op jit(solution)/shard_map/all_gather | solution.py:114
  8.7 11.4 %collective-permute-start.1 = (bf16[30,512]{1,0:T(8,128)(2,1)S(1)}, bf16[30,512]{1,0:T(8,128)(2,1)S(1)}, u32[]{:S(2)}, u32[]{:S(2)}) collective-permute-start(bf16[30,512]{1,0:T(8,128)(2,1)S(1)} %slice_bitcast_fusion), channel_id=1, source_target_pairs={{0,2},{2,4},{4,6},{6,8},{8,10},{10,12},{12,14},{14,16},{16,18},{18... | collective-permute-start | bytes 92168 | tf_op jit(solution)/shard_map/ppermute | solution.py:14
  14.3 5.8 %collective-permute-start = (bf16[30,512]{1,0:T(8,128)(2,1)S(1)}, bf16[30,512]{1,0:T(8,128)(2,1)S(1)}, u32[]{:S(2)}, u32[]{:S(2)}) collective-permute-start(bf16[30,512]{1,0:T(8,128)(2,1)S(1)} %slice_bitcast_fusion.1), channel_id=1, source_target_pairs={{0,2},{2,4},{4,6},{6,8},{8,10},{10,12},{12,14},{14,16},{16,18},{18... | collective-permute-start | bytes 92168 | tf_op jit(solution)/shard_map/ppermute | solution.py:14
  21.8 6.0 %copy-start.9 = (f32[512]{0:T(512)S(1)}, f32[512]{0:T(512)}, u32[]{:S(2)}) copy-start(f32[512]{0:T(512)} %param.11) | copy-start | bytes 6148
  21.8 6.0 %copy-start.10 = (f32[512]{0:T(512)S(1)}, f32[512]{0:T(512)}, u32[]{:S(2)}) copy-start(f32[512]{0:T(512)} %param.12) | copy-start | bytes 6148
  26.8 1.0 copy-start.3
  36.6 3.1 %copy-start.7 = (bf16[1,512,512]{2,1,0:T(8,128)(2,1)S(1)}, bf16[1,512,512]{2,1,0:T(8,128)(2,1)}, u32[]{:S(2)}) copy-start(bf16[1,512,512]{2,1,0:T(8,128)(2,1)} %param.8) | copy-start | bytes 1572868
  39.7 1.2 copy-start.8
  39.7 17.3 %collective-permute-start.3 = (f32[1024,512]{1,0:T(8,128)}, f32[1024,512]{1,0:T(8,128)}, u32[]{:S(2)}, u32[]{:S(2)}) collective-permute-start(f32[1024,512]{1,0:T(8,128)} %dynamic-slice_bitcast_fusion), channel_id=1, source_target_pairs={{0,1},{1,0},{2,3},{3,2},{4,5},{5,4},{6,7},{7,6},{8,9},{9,8},{10,11... | collective-permute-start | bytes 6291464 | tf_op jit(solution)/shard_map/ppermute | solution.py:19
  42.1 4.3 %copy-start.4 = (f32[512,512]{1,0:T(8,128)S(1)}, f32[512,512]{1,0:T(8,128)}, u32[]{:S(2)}) copy-start(f32[512,512]{1,0:T(8,128)} %copy-done.3) | copy-start | bytes 3145732
  49.6 3.8 %copy-start.1 = (f32[512,512]{1,0:T(8,128)}, f32[512,512]{1,0:T(8,128)S(1)}, u32[]{:S(2)}) copy-start(f32[512,512]{1,0:T(8,128)S(1)} %get-tuple-element.41) | copy-start | bytes 3145732
  49.7 17.3 %collective-permute-start.2 = (f32[30,512]{1,0:T(8,128)S(1)}, f32[30,512]{1,0:T(8,128)S(1)}, u32[]{:S(2)}, u32[]{:S(2)}) collective-permute-start(f32[30,512]{1,0:T(8,128)S(1)} %slice.509), channel_id=1, source_target_pairs={{2,0},{4,2},{6,4},{8,6},{10,8},{12,10},{14,12},{16,14},{18,16},{20... | collective-permute-start | bytes 184328 | tf_op jit(solution)/shard_map/ppermute | solution.py:14
  56.4 25.7 %collective-permute-start.28 = (f32[33,512]{1,0:T(8,128)S(1)}, f32[33,512]{1,0:T(8,128)S(1)}, u32[]{:S(2)}, u32[]{:S(2)}) collective-permute-start(f32[33,512]{1,0:T(8,128)S(1)} %broadcast_multiply_fusion), channel_id=1, source_target_pairs={{0,1},{1,0},{2,3},{3,2},{4,5},{5,4},{6,7},{7,6},{8,9},{9,8},{10,11... | collective-permute-start | bytes 202760 | tf_op jit(solution)/shard_map/ppermute | solution.py:19
  59.7 9.1 %copy-start.5 = (f32[542,512]{1,0:T(8,128)S(1)}, f32[542,512]{1,0:T(8,128)}, u32[]{:S(2)}) copy-start(f32[542,512]{1,0:T(8,128)} %maximum_convert_fusion.2) | copy-start | bytes 3330052
  59.7 9.1 %copy-start.6 = (f32[542,512]{1,0:T(8,128)S(1)}, f32[542,512]{1,0:T(8,128)}, u32[]{:S(2)}) copy-start(f32[542,512]{1,0:T(8,128)} %maximum_convert_fusion.1) | copy-start | bytes 3330052
  59.9 8.9 %copy-start.2 = (f32[512,512]{1,0:T(8,128)S(1)}, f32[512,512]{1,0:T(8,128)}, u32[]{:S(2)}) copy-start(f32[512,512]{1,0:T(8,128)} %copy-done.1) | copy-start | bytes 3145732
  59.9 15.0 %collective-permute-start.16 = (bf16[64,512]{1,0:T(8,128)(2,1)S(1)}, bf16[64,512]{1,0:T(8,128)(2,1)S(1)}, u32[]{:S(2)}, u32[]{:S(2)}) collective-permute-start(bf16[64,512]{1,0:T(8,128)(2,1)S(1)} %get-tuple-element.49), channel_id=1, source_target_pairs={{0,24},{2,26},{4,28},{6,30},{8,16},{10,18},{12,20},{14,22},{16,8},... | collective-permute-start | bytes 196616 | tf_op jit(solution)/shard_map/ppermute | solution.py:19
  66.3 8.6 %collective-permute-start.18 = (bf16[64,512]{1,0:T(8,128)(2,1)S(1)}, bf16[64,512]{1,0:T(8,128)(2,1)S(1)}, u32[]{:S(2)}, u32[]{:S(2)}) collective-permute-start(bf16[64,512]{1,0:T(8,128)(2,1)S(1)} %get-tuple-element.50), channel_id=1, source_target_pairs={{0,8},{2,10},{4,12},{6,14},{8,0},{10,2},{12,4},{14,6},{16,24},{18,... | collective-permute-start | bytes 196616 | tf_op jit(solution)/shard_map/ppermute | solution.py:19
  66.3 8.6 %collective-permute-start.17 = (bf16[64,512]{1,0:T(8,128)(2,1)S(1)}, bf16[64,512]{1,0:T(8,128)(2,1)S(1)}, u32[]{:S(2)}, u32[]{:S(2)}) collective-permute-start(bf16[64,512]{1,0:T(8,128)(2,1)S(1)} %get-tuple-element.51), channel_id=1, source_target_pairs={{0,16},{2,18},{4,20},{6,22},{8,24},{10,26},{12,28},{14,30},{16,0},... | collective-permute-start | bytes 196616 | tf_op jit(solution)/shard_map/ppermute | solution.py:19
  67.0 41.4 %collective-permute-start.4 = (bf16[192,512]{1,0:T(8,128)(2,1)S(1)}, bf16[192,512]{1,0:T(8,128)(2,1)S(1)}, u32[]{:S(2)}, u32[]{:S(2)}) collective-permute-start(bf16[192,512]{1,0:T(8,128)(2,1)S(1)} %get-tuple-element.46), channel_id=1, source_target_pairs={{0,6},{2,4},{4,2},{6,0},{8,14},{10,12},{12,10},{14,8},{16,22},{18,... | collective-permute-start | bytes 589832 | tf_op jit(solution)/shard_map/ppermute | solution.py:19
  75.0 4.7 %collective-permute-start.19 = (bf16[16,512]{1,0:T(8,128)(2,1)S(1)}, bf16[16,512]{1,0:T(8,128)(2,1)S(1)}, u32[]{:S(2)}, u32[]{:S(2)}) collective-permute-start(bf16[16,512]{1,0:T(8,128)(2,1)S(1)} %get-tuple-element.55), channel_id=1, source_target_pairs={{0,6},{2,4},{4,2},{6,0},{8,14},{10,12},{12,10},{14,8},{16,22},{18,... | collective-permute-start | bytes 49160 | tf_op jit(solution)/shard_map/ppermute | solution.py:19
  76.2 4.0 %collective-permute-start.21 = (bf16[16,512]{1,0:T(8,128)(2,1)S(1)}, bf16[16,512]{1,0:T(8,128)(2,1)S(1)}, u32[]{:S(2)}, u32[]{:S(2)}) collective-permute-start(bf16[16,512]{1,0:T(8,128)(2,1)S(1)} %get-tuple-element.56), channel_id=1, source_target_pairs={{0,2},{2,0},{4,6},{6,4},{8,10},{10,8},{12,14},{14,12},{16,18},{18,... | collective-permute-start | bytes 49160 | tf_op jit(solution)/shard_map/ppermute | solution.py:19
  77.7 3.7 %collective-permute-start.20 = (bf16[16,512]{1,0:T(8,128)(2,1)S(1)}, bf16[16,512]{1,0:T(8,128)(2,1)S(1)}, u32[]{:S(2)}, u32[]{:S(2)}) collective-permute-start(bf16[16,512]{1,0:T(8,128)(2,1)S(1)} %get-tuple-element.57), channel_id=1, source_target_pairs={{0,4},{2,6},{4,0},{6,2},{8,12},{10,14},{12,8},{14,10},{16,20},{18,... | collective-permute-start | bytes 49160 | tf_op jit(solution)/shard_map/ppermute | solution.py:19
  79.7 28.7 %collective-permute-start.6 = (bf16[192,512]{1,0:T(8,128)(2,1)S(1)}, bf16[192,512]{1,0:T(8,128)(2,1)S(1)}, u32[]{:S(2)}, u32[]{:S(2)}) collective-permute-start(bf16[192,512]{1,0:T(8,128)(2,1)S(1)} %get-tuple-element.47), channel_id=1, source_target_pairs={{0,2},{2,0},{4,6},{6,4},{8,10},{10,8},{12,14},{14,12},{16,18},{18,... | collective-permute-start | bytes 589832 | tf_op jit(solution)/shard_map/ppermute | solution.py:19
  81.5 4.9 %collective-permute-start.24 = (bf16[16,512]{1,0:T(8,128)(2,1)S(1)}, bf16[16,512]{1,0:T(8,128)(2,1)S(1)}, u32[]{:S(2)}, u32[]{:S(2)}) collective-permute-start(bf16[16,512]{1,0:T(8,128)(2,1)S(1)} %fusion.129), channel_id=1, source_target_pairs={{0,2},{2,0},{4,6},{6,4},{8,10},{10,8},{12,14},{14,12},{16,18},{18,... | collective-permute-start | bytes 49160 | tf_op jit(solution)/shard_map/ppermute | solution.py:19
  82.1 9.8 %collective-permute-start.31 = (f32[33,512]{1,0:T(8,128)S(1)}, f32[33,512]{1,0:T(8,128)S(1)}, u32[]{:S(2)}, u32[]{:S(2)}) collective-permute-start(f32[33,512]{1,0:T(8,128)S(1)} %fusion.134), channel_id=1, source_target_pairs={{0,6},{2,4},{4,2},{6,0},{8,14},{10,12},{12,10},{14,8},{16,22},{18,... | collective-permute-start | bytes 202760 | tf_op jit(solution)/shard_map/ppermute | solution.py:19
  83.9 4.5 %collective-permute-start.23 = (bf16[16,512]{1,0:T(8,128)(2,1)S(1)}, bf16[16,512]{1,0:T(8,128)(2,1)S(1)}, u32[]{:S(2)}, u32[]{:S(2)}) collective-permute-start(bf16[16,512]{1,0:T(8,128)(2,1)S(1)} %fusion.129), channel_id=1, source_target_pairs={{0,4},{2,6},{4,0},{6,2},{8,12},{10,14},{12,8},{14,10},{16,20},{18,... | collective-permute-start | bytes 49160 | tf_op jit(solution)/shard_map/ppermute | solution.py:19
  86.4 4.8 %collective-permute-start.22 = (bf16[16,512]{1,0:T(8,128)(2,1)S(1)}, bf16[16,512]{1,0:T(8,128)(2,1)S(1)}, u32[]{:S(2)}, u32[]{:S(2)}) collective-permute-start(bf16[16,512]{1,0:T(8,128)(2,1)S(1)} %fusion.129), channel_id=1, source_target_pairs={{0,6},{2,4},{4,2},{6,0},{8,14},{10,12},{12,10},{14,8},{16,22},{18,... | collective-permute-start | bytes 49160 | tf_op jit(solution)/shard_map/ppermute | solution.py:19
  88.4 4.8 %collective-permute-start.30 = (f32[33,512]{1,0:T(8,128)S(1)}, f32[33,512]{1,0:T(8,128)S(1)}, u32[]{:S(2)}, u32[]{:S(2)}) collective-permute-start(f32[33,512]{1,0:T(8,128)S(1)} %fusion.134), channel_id=1, source_target_pairs={{0,4},{2,6},{4,0},{6,2},{8,12},{10,14},{12,8},{14,10},{16,20},{18,... | collective-permute-start | bytes 202760 | tf_op jit(solution)/shard_map/ppermute | solution.py:19
  91.2 4.4 %collective-permute-start.29 = (f32[33,512]{1,0:T(8,128)S(1)}, f32[33,512]{1,0:T(8,128)S(1)}, u32[]{:S(2)}, u32[]{:S(2)}) collective-permute-start(f32[33,512]{1,0:T(8,128)S(1)} %fusion.134), channel_id=1, source_target_pairs={{0,2},{2,0},{4,6},{6,4},{8,10},{10,8},{12,14},{14,12},{16,18},{18,... | collective-permute-start | bytes 202760 | tf_op jit(solution)/shard_map/ppermute | solution.py:19
  91.9 16.5 %collective-permute-start.5 = (bf16[192,512]{1,0:T(8,128)(2,1)S(1)}, bf16[192,512]{1,0:T(8,128)(2,1)S(1)}, u32[]{:S(2)}, u32[]{:S(2)}) collective-permute-start(bf16[192,512]{1,0:T(8,128)(2,1)S(1)} %get-tuple-element.48), channel_id=1, source_target_pairs={{0,4},{2,6},{4,0},{6,2},{8,12},{10,14},{12,8},{14,10},{16,20},{18,... | collective-permute-start | bytes 589832 | tf_op jit(solution)/shard_map/ppermute | solution.py:19
  93.2 4.7 %collective-permute-start.27 = (bf16[64,512]{1,0:T(8,128)(2,1)S(1)}, bf16[64,512]{1,0:T(8,128)(2,1)S(1)}, u32[]{:S(2)}, u32[]{:S(2)}) collective-permute-start(bf16[64,512]{1,0:T(8,128)(2,1)S(1)} %maximum_select_fusion.9), channel_id=1, source_target_pairs={{0,8},{2,10},{4,12},{6,14},{8,0},{10,2},{12,4},{14,6},{16,24},{18,... | collective-permute-start | bytes 196616 | tf_op jit(solution)/shard_map/ppermute | solution.py:19
  95.6 5.6 %collective-permute-start.26 = (bf16[64,512]{1,0:T(8,128)(2,1)S(1)}, bf16[64,512]{1,0:T(8,128)(2,1)S(1)}, u32[]{:S(2)}, u32[]{:S(2)}) collective-permute-start(bf16[64,512]{1,0:T(8,128)(2,1)S(1)} %maximum_select_fusion.9), channel_id=1, source_target_pairs={{0,16},{2,18},{4,20},{6,22},{8,24},{10,26},{12,28},{14,30},{16,0},... | collective-permute-start | bytes 196616 | tf_op jit(solution)/shard_map/ppermute | solution.py:19
  97.9 9.9 %collective-permute-start.25 = (bf16[64,512]{1,0:T(8,128)(2,1)S(1)}, bf16[64,512]{1,0:T(8,128)(2,1)S(1)}, u32[]{:S(2)}, u32[]{:S(2)}) collective-permute-start(bf16[64,512]{1,0:T(8,128)(2,1)S(1)} %maximum_select_fusion.9), channel_id=1, source_target_pairs={{0,24},{2,26},{4,28},{6,30},{8,16},{10,18},{12,20},{14,22},{16,8},... | collective-permute-start | bytes 196616 | tf_op jit(solution)/shard_map/ppermute | solution.py:19
  101.2 16.3 %collective-permute-start.34 = (f32[33,512]{1,0:T(8,128)S(1)}, f32[33,512]{1,0:T(8,128)S(1)}, u32[]{:S(2)}, u32[]{:S(2)}) collective-permute-start(f32[33,512]{1,0:T(8,128)S(1)} %add_add_fusion.1), channel_id=1, source_target_pairs={{0,24},{2,26},{4,28},{6,30},{8,16},{10,18},{12,20},{14,22},{16,8},... | collective-permute-start | bytes 202760 | tf_op jit(solution)/shard_map/ppermute | solution.py:19
  107.9 9.7 %collective-permute-start.33 = (f32[33,512]{1,0:T(8,128)S(1)}, f32[33,512]{1,0:T(8,128)S(1)}, u32[]{:S(2)}, u32[]{:S(2)}) collective-permute-start(f32[33,512]{1,0:T(8,128)S(1)} %add_add_fusion.1), channel_id=1, source_target_pairs={{0,16},{2,18},{4,20},{6,22},{8,24},{10,26},{12,28},{14,30},{16,0},... | collective-permute-start | bytes 202760 | tf_op jit(solution)/shard_map/ppermute | solution.py:19
  108.6 6.0 %collective-permute-start.7 = (bf16[48,512]{1,0:T(8,128)(2,1)S(1)}, bf16[48,512]{1,0:T(8,128)(2,1)S(1)}, u32[]{:S(2)}, u32[]{:S(2)}) collective-permute-start(bf16[48,512]{1,0:T(8,128)(2,1)S(1)} %get-tuple-element.52), channel_id=1, source_target_pairs={{0,24},{2,26},{4,28},{6,30},{8,16},{10,18},{12,20},{14,22},{16,8},... | collective-permute-start | bytes 147464 | tf_op jit(solution)/shard_map/ppermute | solution.py:19
  109.1 6.9 %collective-permute-start.9 = (bf16[48,512]{1,0:T(8,128)(2,1)S(1)}, bf16[48,512]{1,0:T(8,128)(2,1)S(1)}, u32[]{:S(2)}, u32[]{:S(2)}) collective-permute-start(bf16[48,512]{1,0:T(8,128)(2,1)S(1)} %get-tuple-element.53), channel_id=1, source_target_pairs={{0,8},{2,10},{4,12},{6,14},{8,0},{10,2},{12,4},{14,6},{16,24},{18,... | collective-permute-start | bytes 147464 | tf_op jit(solution)/shard_map/ppermute | solution.py:19
  111.6 5.8 %collective-permute-start.8 = (bf16[48,512]{1,0:T(8,128)(2,1)S(1)}, bf16[48,512]{1,0:T(8,128)(2,1)S(1)}, u32[]{:S(2)}, u32[]{:S(2)}) collective-permute-start(bf16[48,512]{1,0:T(8,128)(2,1)S(1)} %get-tuple-element.54), channel_id=1, source_target_pairs={{0,16},{2,18},{4,20},{6,22},{8,24},{10,26},{12,28},{14,30},{16,0},... | collective-permute-start | bytes 147464 | tf_op jit(solution)/shard_map/ppermute | solution.py:19
  114.5 4.4 %collective-permute-start.32 = (f32[33,512]{1,0:T(8,128)S(1)}, f32[33,512]{1,0:T(8,128)S(1)}, u32[]{:S(2)}, u32[]{:S(2)}) collective-permute-start(f32[33,512]{1,0:T(8,128)S(1)} %add_add_fusion.1), channel_id=1, source_target_pairs={{0,8},{2,10},{4,12},{6,14},{8,0},{10,2},{12,4},{14,6},{16,24},{18,... | collective-permute-start | bytes 202760 | tf_op jit(solution)/shard_map/ppermute | solution.py:19
  117.4 5.4 %collective-permute-start.12 = (bf16[48,512]{1,0:T(8,128)(2,1)S(1)}, bf16[48,512]{1,0:T(8,128)(2,1)S(1)}, u32[]{:S(2)}, u32[]{:S(2)}) collective-permute-start(bf16[48,512]{1,0:T(8,128)(2,1)S(1)} %fusion.120), channel_id=1, source_target_pairs={{0,8},{2,10},{4,12},{6,14},{8,0},{10,2},{12,4},{14,6},{16,24},{18,... | collective-permute-start | bytes 147464 | tf_op jit(solution)/shard_map/ppermute | solution.py:19
  119.0 5.1 %collective-permute-start.11 = (bf16[48,512]{1,0:T(8,128)(2,1)S(1)}, bf16[48,512]{1,0:T(8,128)(2,1)S(1)}, u32[]{:S(2)}, u32[]{:S(2)}) collective-permute-start(bf16[48,512]{1,0:T(8,128)(2,1)S(1)} %fusion.120), channel_id=1, source_target_pairs={{0,16},{2,18},{4,20},{6,22},{8,24},{10,26},{12,28},{14,30},{16,0},... | collective-permute-start | bytes 147464 | tf_op jit(solution)/shard_map/ppermute | solution.py:19
  120.2 5.9 %collective-permute-start.10 = (bf16[48,512]{1,0:T(8,128)(2,1)S(1)}, bf16[48,512]{1,0:T(8,128)(2,1)S(1)}, u32[]{:S(2)}, u32[]{:S(2)}) collective-permute-start(bf16[48,512]{1,0:T(8,128)(2,1)S(1)} %fusion.120), channel_id=1, source_target_pairs={{0,24},{2,26},{4,28},{6,30},{8,16},{10,18},{12,20},{14,22},{16,8},... | collective-permute-start | bytes 147464 | tf_op jit(solution)/shard_map/ppermute | solution.py:19
  126.2 5.7 %collective-permute-start.15 = (bf16[192,512]{1,0:T(8,128)(2,1)S(1)}, bf16[192,512]{1,0:T(8,128)(2,1)S(1)}, u32[]{:S(2)}, u32[]{:S(2)}) collective-permute-start(bf16[192,512]{1,0:T(8,128)(2,1)S(1)} %maximum_select_fusion.4), channel_id=1, source_target_pairs={{0,2},{2,0},{4,6},{6,4},{8,10},{10,8},{12,14},{14,12},{16,18},{18,... | collective-permute-start | bytes 589832 | tf_op jit(solution)/shard_map/ppermute | solution.py:19
  127.2 5.7 %collective-permute-start.14 = (bf16[192,512]{1,0:T(8,128)(2,1)S(1)}, bf16[192,512]{1,0:T(8,128)(2,1)S(1)}, u32[]{:S(2)}, u32[]{:S(2)}) collective-permute-start(bf16[192,512]{1,0:T(8,128)(2,1)S(1)} %maximum_select_fusion.4), channel_id=1, source_target_pairs={{0,4},{2,6},{4,0},{6,2},{8,12},{10,14},{12,8},{14,10},{16,20},{18,... | collective-permute-start | bytes 589832 | tf_op jit(solution)/shard_map/ppermute | solution.py:19
  128.2 6.8 %collective-permute-start.13 = (bf16[192,512]{1,0:T(8,128)(2,1)S(1)}, bf16[192,512]{1,0:T(8,128)(2,1)S(1)}, u32[]{:S(2)}, u32[]{:S(2)}) collective-permute-start(bf16[192,512]{1,0:T(8,128)(2,1)S(1)} %maximum_select_fusion.4), channel_id=1, source_target_pairs={{0,6},{2,4},{4,2},{6,0},{8,14},{10,12},{12,10},{14,8},{16,22},{18,... | collective-permute-start | bytes 589832 | tf_op jit(solution)/shard_map/ppermute | solution.py:19
Sparse Core Ops, SparseCore 0:
  9.5 13.2 all-gather.1

commit v2 on v1

v2 whole, which is shorter than its diff:
```python
import functools
import math

import jax
import jax.numpy as jnp
from jax import lax
from jax.experimental import pallas as pl
from jax.experimental.pallas import tpu as pltpu
from jax.sharding import PartitionSpec as P

epsilon = 1e-06


def exchange(value, axis, offset):
    count = lax.axis_size(axis)
    return lax.ppermute(value, axis, [(i, i ^ offset) for i in range(count)])


def levels_of(count):
    bits = count.bit_length() - 1
    return [(1 << low, 1 << min(2, bits - low)) for low in range(0, bits, 2)]


def digit(level):
    low, width = level
    return (lax.axis_index("sp") // low) % width


def reduce_level(total, level):
    low, width = level
    mine = digit(level)
    parts = total.reshape((width, total.shape[0] // width) + total.shape[1:])
    arrived = [
        exchange(
            lax.dynamic_index_in_dim(parts, mine ^ other, 0, False).astype(jnp.bfloat16),
            "sp",
            other * low,
        )
        for other in range(width - 1, 0, -1)
    ]
    kept = lax.dynamic_index_in_dim(parts, mine, 0, False)
    for part in arrived:
        kept = kept + part.astype(jnp.float32)
    return kept


def gather_level(rows, level):
    low, width = level
    mine = digit(level)
    pieces = [rows] + [None] * (width - 1)
    for other in range(width - 1, 0, -1):
        pieces[other] = exchange(rows, "sp", other * low)
    half = 1
    while half < width:
        swap = (mine // half) % 2 == 1
        paired = []
        for i in range(0, len(pieces), 2):
            first, second = pieces[i], pieces[i + 1]
            paired.append(
                jnp.where(
                    swap,
                    jnp.concatenate([second, first], axis=0),
                    jnp.concatenate([first, second], axis=0),
                )
            )
        pieces = paired
        half *= 2
    return pieces[0]


def tree(items):
    while len(items) > 1:
        items = [items[i] + items[i + 1] for i in range(0, len(items), 2)]
    return items[0]


def all_sum(value, axis, level):
    low, width = level
    return tree([value] + [exchange(value, axis, other * low) for other in range(1, width)])


lanes = 128
sublanes = 8


def rounded_up(count, unit):
    return -(-count // unit) * unit


def fwd_kernel(value, gate, halo, cotan, weight, gain, shift, *rest, taps, pad, seg, eps, scale, others):
    sent = rest[: 1 if others else 0]
    own, gated, normed, inv_out, taps_in, conv, act, cot, arrive = rest[1 if others else 0 :]
    length, channels = value.shape
    groups = channels // lanes
    segments = length // seg
    rows = pad + seg
    copy = pltpu.make_async_copy(cotan, cot, arrive)
    copy.start()

    def gate_rows(v, g):
        return v.astype(jnp.float32) * jax.nn.sigmoid(g.astype(jnp.float32))

    for k in range(groups):
        cols = slice(k * lanes, (k + 1) * lanes)
        gated[k * rows : k * rows + pad, :] = gate_rows(halo[:pad, cols], halo[pad:, cols])
        for s in range(segments):
            at = (s * groups + k) * rows + pad
            block = gate_rows(value[s * seg : (s + 1) * seg, cols], gate[s * seg : (s + 1) * seg, cols])
            gated[at : at + seg, :] = block
            if s + 1 < segments:
                to = ((s + 1) * groups + k) * rows
                gated[to : to + pad, :] = block[seg - pad :]
            taps_in[(s * groups + k) * pad : (s * groups + k) * pad + taps, :] = weight[:, cols]
    tap = [taps_in[pl.ds(j, sublanes, stride=pad), :] for j in range(taps)]
    unit = 8

    def conv_block(i, carry):
        base = i * unit
        sums = [None] * unit
        for m in range(unit + taps - 1):
            row = gated[pl.ds(base + (pad - taps + 1) + m, sublanes, stride=rows), :]
            for u in range(unit):
                j = m - u
                if 0 <= j < taps:
                    term = tap[j] * row
                    sums[u] = term if sums[u] is None else sums[u] + term
        for u in range(unit):
            conv[pl.ds(base + u, sublanes, stride=seg), :] = sums[u]
        return carry

    lax.fori_loop(0, seg // unit, conv_block, 0)
    chunk = 32
    for s in range(segments):

        def norm_block(i, carry, s=s):
            base = pl.multiple_of(i * chunk, chunk)
            out = pl.multiple_of(s * seg + i * chunk, chunk)
            parts = [conv[pl.ds((s * groups + k) * seg + base, chunk), :] for k in range(groups)]
            mean = jnp.sum(sum(parts), axis=-1, keepdims=True) / channels
            parts = [p - mean for p in parts]
            var = jnp.sum(sum(p * p for p in parts), axis=-1, keepdims=True) / channels
            inv = lax.rsqrt(var + eps)
            inv_out[pl.ds(out, chunk), :] = jnp.broadcast_to(inv, (chunk, lanes))
            for k in range(groups):
                cols = slice(k * lanes, (k + 1) * lanes)
                n = parts[k] * inv
                normed[pl.ds(out, chunk), cols] = n
                pre = n * gain[:, cols] + shift[:, cols]
                act[pl.ds(out, chunk), cols] = (pre * jax.nn.sigmoid(pre)).astype(jnp.bfloat16)
            return carry

        lax.fori_loop(0, seg // chunk, norm_block, 0)
    copy.wait()
    features = own.shape[0]
    index = lax.axis_index("dp")
    step = min(features, 256)
    for other in list(range(1, others + 1)) + [0]:
        for f in range(0, features, step):
            at = pl.multiple_of((index ^ other) * features + f, lanes)
            part = lax.dot_general(
                cot[:, pl.ds(at, step)],
                act[...],
                (((0,), (0,)), ((), ())),
                preferred_element_type=jnp.float32,
            )
            if other:
                sent[0][other - 1, f : f + step, :] = part * scale
            else:
                own[f : f + step, :] = part * scale


def bwd_kernel(cotan, normed, inv_in, gain, shift, *rest, seg, scale, pieces):
    weights = rest[:pieces]
    grads, head, sums, act = rest[pieces:]
    length, channels = normed.shape
    groups = channels // lanes
    segments = length // seg
    features = weights[0].shape[0]
    index = lax.axis_index("dp")
    for other in range(pieces):
        at = pl.multiple_of((index ^ other) * features, lanes)
        part = jnp.dot(
            cotan[:, pl.ds(at, features)], weights[other][...], preferred_element_type=jnp.float32
        )
        act[...] = part if other == 0 else act[...] + part
    chunk = 32
    total = tuple(jnp.zeros((sublanes, lanes), jnp.float32) for _ in range(2 * groups))
    for s in range(segments):

        def grad_block(i, carry, s=s):
            base = pl.multiple_of(i * chunk, chunk)
            at = pl.multiple_of(s * seg + i * chunk, chunk)
            inv = inv_in[pl.ds(at, chunk), :]
            carry = list(carry)
            n, gn = [], []
            for k in range(groups):
                cols = slice(k * lanes, (k + 1) * lanes)
                nk = normed[pl.ds(at, chunk), cols]
                pre = nk * gain[:, cols] + shift[:, cols]
                sig = jax.nn.sigmoid(pre)
                grad_pre = act[pl.ds(at, chunk), cols] * sig * (1.0 + pre * (1.0 - sig))
                by_gain = (grad_pre * nk).reshape(chunk // sublanes, sublanes, lanes)
                by_shift = grad_pre.reshape(chunk // sublanes, sublanes, lanes)
                carry[k] = carry[k] + jnp.sum(by_gain, axis=0)
                carry[groups + k] = carry[groups + k] + jnp.sum(by_shift, axis=0)
                n.append(nk)
                gn.append(grad_pre * gain[:, cols])
            mean = jnp.sum(sum(gn), axis=-1, keepdims=True) / channels
            slope = jnp.sum(sum(a * b for a, b in zip(gn, n)), axis=-1, keepdims=True) / channels
            for k in range(groups):
                grads[pl.ds((s * groups + k) * seg + base, chunk), :] = inv * (
                    gn[k] - mean - n[k] * slope
                )
            return tuple(carry)

        total = lax.fori_loop(0, seg // chunk, grad_block, total)
    pad = head.shape[0]
    for k in range(groups):
        cols = slice(k * lanes, (k + 1) * lanes)
        head[:, cols] = grads[k * seg : k * seg + pad, :]
        for row in range(2):
            sums[row : row + 1, cols] = (
                jnp.sum(total[row * groups + k], axis=0, keepdims=True) * scale
            )


def taps_kernel(grads, gated, sums, small, spread, *, taps, pad, seg, scale):
    rows = pad + seg
    groups = small.shape[1] // lanes
    unit = 4

    def tap_block(i, carry):
        base = i * unit
        carry = list(carry)
        grad = [grads[pl.ds(base + u, sublanes, stride=seg), :] for u in range(unit)]
        for m in range(unit + taps - 1):
            row = gated[pl.ds(base + (pad - taps + 1) + m, sublanes, stride=rows), :]
            for u in range(unit):
                j = m - u
                if 0 <= j < taps:
                    carry[j] = carry[j] + grad[u] * row
        return tuple(carry)

    zero = jnp.zeros((sublanes, lanes), jnp.float32)
    total = lax.fori_loop(0, seg // unit, tap_block, (zero,) * taps)
    for j in range(taps):
        spread[pl.ds(j, sublanes, stride=pad), :] = total[j] * scale
    small[...] = jnp.zeros_like(small)
    for k in range(groups):
        cols = slice(k * lanes, (k + 1) * lanes)
        small[:taps, cols] = sum(
            spread[b * pad : b * pad + taps, :] for b in range(k, sublanes, groups)
        )
        small[taps : taps + 2, cols] = sums[:, cols]


def input_kernel(grads, halo, weight, value, gate, grad_value, grad_gate, taps_in, tail, conv, *, taps, pad, seg):
    length, channels = value.shape
    groups = channels // lanes
    segments = length // seg
    for k in range(groups):
        cols = slice(k * lanes, (k + 1) * lanes)
        for s in range(segments):
            b = s * groups + k
            taps_in[b * pad : b * pad + taps, :] = weight[:, cols]
            tail[b * 2 * pad : b * 2 * pad + pad, :] = grads[(b + 1) * seg - pad : (b + 1) * seg, :]
            if s + 1 < segments:
                after = grads[(b + groups) * seg : (b + groups) * seg + pad, :]
            else:
                after = halo[:, cols]
            tail[b * 2 * pad + pad : (b + 1) * 2 * pad, :] = after
    tap = [taps_in[pl.ds(j, sublanes, stride=pad), :] for j in range(taps)]
    unit = 8

    def block_of(source, stride, offset):
        def conv_block(i, carry):
            base = i * unit
            sums = [None] * unit
            for m in range(unit + taps - 1):
                row = source[pl.ds(base + m, sublanes, stride=stride), :]
                for u in range(unit):
                    j = taps - 1 - (m - u)
                    if 0 <= j < taps:
                        term = tap[j] * row
                        sums[u] = term if sums[u] is None else sums[u] + term
            for u in range(unit):
                conv[pl.ds(offset + base + u, sublanes, stride=seg), :] = sums[u]
            return carry

        return conv_block

    lax.fori_loop(0, (seg - pad) // unit, block_of(grads, seg, 0), 0)
    lax.fori_loop(0, pad // unit, block_of(tail, 2 * pad, seg - pad), 0)
    chunk = 32
    for s in range(segments):

        def out_block(i, carry, s=s):
            base = pl.multiple_of(i * chunk, chunk)
            at = pl.multiple_of(s * seg + i * chunk, chunk)
            for k in range(groups):
                cols = slice(k * lanes, (k + 1) * lanes)
                grad = conv[pl.ds((s * groups + k) * seg + base, chunk), :]
                sig = jax.nn.sigmoid(gate[pl.ds(at, chunk), cols].astype(jnp.float32))
                by_value = grad * sig
                grad_value[pl.ds(at, chunk), cols] = by_value.astype(jnp.bfloat16)
                grad_gate[pl.ds(at, chunk), cols] = (
                    by_value * value[pl.ds(at, chunk), cols].astype(jnp.float32) * (1.0 - sig)
                ).astype(jnp.bfloat16)
            return carry

        lax.fori_loop(0, seg // chunk, out_block, 0)


def in_vmem(count):
    return [pl.BlockSpec(memory_space=pltpu.VMEM)] * count


def f32(*shape):
    return jax.ShapeDtypeStruct(shape, jnp.float32)


def per_device(glu_value, glu_gate, cotangent, conv_weight, norm_gain, norm_shift, out_weight):
    value_rows = glu_value[0]
    gate_rows = glu_gate[0]
    cotan_rows = cotangent[0]
    length, channels = value_rows.shape
    taps = conv_weight.shape[0]
    features = out_weight.shape[0]
    count_sp = lax.axis_size("sp")
    count_dp = lax.axis_size("dp")
    scale = 1.0 / math.sqrt(length * count_sp * count_dp)
    pad = rounded_up(taps, 16)
    seg = length * (channels // lanes) // sublanes
    gain = norm_gain[None]
    shift = norm_shift[None]
    blocks = length // seg * (channels // lanes)

    weights = [out_weight] + [exchange(out_weight, "dp", k) for k in range(1, count_dp)]
    halo = lax.ppermute(
        jnp.concatenate([value_rows[length - pad :], gate_rows[length - pad :]], axis=0),
        "sp",
        [(i, i + 1) for i in range(count_sp - 1)],
    )
    others = count_dp - 1
    sent_shape = [f32(others, features, channels)] if others else []
    outs = pl.pallas_call(
        functools.partial(
            fwd_kernel, taps=taps, pad=pad, seg=seg, eps=epsilon, scale=scale, others=others
        ),
        out_shape=sent_shape
        + [
            f32(features, channels),
            f32(blocks * (pad + seg), lanes),
            f32(length, channels),
            f32(length, lanes),
        ],
        in_specs=in_vmem(3) + [pl.BlockSpec(memory_space=pl.ANY)] + in_vmem(3),
        out_specs=in_vmem(len(sent_shape) + 4),
        scratch_shapes=[
            pltpu.VMEM((blocks * pad, lanes), jnp.float32),
            pltpu.VMEM((blocks * seg, lanes), jnp.float32),
            pltpu.VMEM((length, channels), jnp.bfloat16),
            pltpu.VMEM(cotan_rows.shape, jnp.bfloat16),
            pltpu.SemaphoreType.DMA,
        ],
        name="forward",
    )(value_rows, gate_rows, halo, cotan_rows, conv_weight, gain, shift)
    own, gated, normed, inv = outs[-4:]
    arrived = [exchange(outs[0][k - 1], "dp", k) for k in range(1, count_dp)]

    grads, head, sums = pl.pallas_call(
        functools.partial(bwd_kernel, seg=seg, scale=scale, pieces=count_dp),
        out_shape=[f32(blocks * seg, lanes), f32(pad, channels), f32(2, channels)],
        in_specs=in_vmem(5 + count_dp),
        out_specs=in_vmem(3),
        scratch_shapes=[pltpu.VMEM((length, channels), jnp.float32)],
        name="backward",
    )(cotan_rows, normed, inv, gain, shift, *weights)
    later = lax.ppermute(head, "sp", [(i, i - 1) for i in range(1, count_sp)])
    small = pl.pallas_call(
        functools.partial(taps_kernel, taps=taps, pad=pad, seg=seg, scale=scale),
        out_shape=f32(rounded_up(taps + 2, 8), channels),
        in_specs=in_vmem(3),
        out_specs=in_vmem(1)[0],
        scratch_shapes=[pltpu.VMEM((blocks * pad, lanes), jnp.float32)],
        name="taps",
    )(grads, gated, sums)
    grad_value, grad_gate = pl.pallas_call(
        functools.partial(input_kernel, taps=taps, pad=pad, seg=seg),
        out_shape=[jax.ShapeDtypeStruct((length, channels), jnp.bfloat16)] * 2,
        in_specs=in_vmem(5),
        out_specs=in_vmem(2),
        scratch_shapes=[
            pltpu.VMEM((blocks * pad, lanes), jnp.float32),
            pltpu.VMEM((blocks * 2 * pad, lanes), jnp.float32),
            pltpu.VMEM((blocks * seg, lanes), jnp.float32),
        ],
        name="inputs",
    )(grads, later, conv_weight, value_rows, gate_rows)

    levels = levels_of(count_sp)
    total = tree([own] + arrived)
    cut = 3 * features // 4
    if len(levels) > 1 and cut % (16 * count_sp) == 0 and (features - cut) % (16 * count_sp) == 0:
        colours = [(total[:cut], levels), (total[cut:], levels[1:] + levels[:1])]
    else:
        colours = [(total, levels)]
    states = [c[0] for c in colours]
    for step in range(len(levels)):
        states = [reduce_level(v, order[step]) for v, (_, order) in zip(states, colours)]
    states = [v.astype(jnp.bfloat16) for v in states]
    small = all_sum(small, "dp", (1, count_dp))
    for step in reversed(range(len(levels))):
        states = [gather_level(v, order[step]) for v, (_, order) in zip(states, colours)]
        small = all_sum(small, "sp", levels[len(levels) - 1 - step])
    grad_out_weight = jnp.concatenate(states, axis=0).astype(jnp.float32)
    return (
        grad_value[None],
        grad_gate[None],
        grad_out_weight,
        small[:taps],
        small[taps],
        small[taps + 1],
    )


def solution(mesh):
    in_specs = (
        P("dp", "sp", None),
        P("dp", "sp", None),
        P("dp", "sp", None),
        P(),
        P(),
        P(),
        P("dp", None),
    )
    out_specs = (P("dp", "sp", None), P("dp", "sp", None), P("dp", None), P(), P(), P())
    return jax.shard_map(
        per_device, mesh=mesh, in_specs=in_specs, out_specs=out_specs, check_vma=False
    )
```

time: 145 us -> 132 us (0.910)
  Pallas kernels: 0 us -> 34.7 us
  other arithmetic: 27.3 us -> 5.59 us
  waiting for transfers between devices: 18.4 us -> 36.5 us
  between operations: 14.6 us -> 1.06 us
  local copies, waits for them, and re-layouts: 17.4 us -> 4.72 us
  starting transfers between devices: 58.4 us -> 48.6 us
  matrix products: 7.77 us -> 0 us
    pallas_call x0 -> x4, Pallas kernels: none -> 34.7 us  [the longest x1 12.2 us: per_device(): pl.pallas_call(functools.partial(fwd_kernel, taps=taps, pad=pad, seg=seg,...]
    ppermute x32 -> x33, waiting for transfers between devices: 17.7 us -> 29.9 us  [exchange(): return lax.ppermute(value, axis, [(i, i ^ offset) for i in range(count)])]
    reduce_sum x4 -> x0, other arithmetic: 10.8 us -> none  [the longest x2 5.52 us: per_device(): jnp.sum(grad_conv_rows * gated_ext[offset:offset + length], axis=0)]
    dot_general x2 -> x0, matrix products: 7.77 us -> none  [the longest x1 4.33 us: per_device(): jnp.dot(columns, lax.all_gather(out_weight, 'dp', axis=0, tiled=True), pr...]
    broadcast_in_dim x2 -> x0, other arithmetic: 7.18 us -> none  [the longest x1 6.09 us: per_device(): grad_gate[None]]
    ppermute x3 -> x2, waiting for transfers between devices: 0.01 us -> 6.58 us  [the longest x1 4.69 us: per_device(): later = lax.ppermute(head, 'sp', [(i, i - 1) for i in range(1, count_sp)])]
    ppermute x32 -> x33, starting transfers between devices: 48.6 us -> 42.5 us  [exchange(): return lax.ppermute(value, axis, [(i, i ^ offset) for i in range(count)])]
    reshape x1 -> x0, local copies, waits for them, and re-layouts: 5.35 us -> none  [per_device(): blocks = (product * scale).reshape(count_dp, features, channels)]
  transfers between devices with their start and end apart: 36 -> 35, of which waited for: 14 -> 16; matrix products, arithmetic and copies ran while one was open for 34% -> 4% of each run, Pallas kernels for 0% -> 17%
where the time goes in v2:
time: 132 us; the launch traced here: 131 us
  starting transfers between devices  48.6 us (37%)
  waiting for transfers between devices  36.5 us (28%)
  Pallas kernels  34.7 us (26%)
  other arithmetic  5.59 us (4%)
  local copies, waits for them, and re-layouts  4.72 us (4%)
    ppermute x33, starting transfers between devices, exchange(): return lax.ppermute(value, axis, [(i, i ^ offset) for i in range(count)])  42.5 us
    ppermute x33, waiting for transfers between devices, exchange(): return lax.ppermute(value, axis, [(i, i ^ offset) for i in range(count)])  29.9 us
    pallas_call x1, Pallas kernels, per_device(): pl.pallas_call(functools.partial(fwd_kernel, taps=taps, pad=pad, seg=seg,...  12.2 us
    pallas_call x1, Pallas kernels, per_device(): pl.pallas_call(functools.partial(taps_kernel, taps=taps, pad=pad, seg=seg...  8.17 us
    pallas_call x1, Pallas kernels, per_device(): pl.pallas_call(functools.partial(input_kernel, taps=taps, pad=pad, seg=se...  7.55 us
    pallas_call x1, Pallas kernels, per_device(): pl.pallas_call(functools.partial(bwd_kernel, seg=seg, scale=scale, pieces...  6.82 us
    ppermute x1, starting transfers between devices, per_device(): lax.ppermute(jnp.concatenate([value_rows[length - pad:], gate_rows[length...  4.87 us
    ppermute x1, waiting for transfers between devices, per_device(): later = lax.ppermute(head, 'sp', [(i, i - 1) for i in range(1, count_sp)])  4.69 us
  transfers between devices with their start and end apart: 35, of which 16 were waited for; matrix products, arithmetic and copies ran while one was open for 4% of the time, Pallas kernels for 17%

profile of v2, /device:TPU:0, one launch (start us, length us, event | category | flops | bytes accessed | tf_op | source)
XLA Modules:
  0.0 131.2 jit_solution(3164089607846829326)
XLA Ops:
  0.6 0.9 slice_bitcast_fusion
  1.5 4.9 %collective-permute-start = (bf16[64,512]{1,0:T(8,128)(2,1)S(1)}, bf16[64,512]{1,0:T(8,128)(2,1)S(1)}, u32[]{:S(2)}, u32[]{:S(2)}) collective-permute-start(bf16[64,512]{1,0:T(8,128)(2,1)S(1)} %pad_maximum_fusion), channel_id=1, source_target_pairs={{0,2},{2,4},{4,6},{6,8},{8,10},{10,12},{12,14},{14,16},{16,18},{18... | collective-permute-start | bytes 196616 | tf_op jit(solution)/shard_map/ppermute | solution.py:339
  6.4 1.9 %collective-permute-done.halo = bf16[64,512]{1,0:T(8,128)(2,1)S(1)} collective-permute-done((bf16[64,512]{1,0:T(8,128)(2,1)S(1)}, bf16[64,512]{1,0:T(8,128)(2,1)S(1)}, u32[]{:S(2)}, u32[]{:S(2)}) %collective-permute-start) | collective-permute-done | bytes 65568 | tf_op jit(solution)/shard_map/ppermute | solution.py:339
  8.9 12.2 %forward.1 = (f32[1,1024,512]{2,1,0:T(8,128)}, f32[1024,512]{1,0:T(8,128)}, f32[2304,128]{1,0:T(8,128)}, f32[512,512]{1,0:T(8,128)}, f32[512,128]{1,0:T(8,128)}) custom-call(bf16[512,512]{1,0:T(8,128)(2,1)} %bitcast.74, bf16[512,512]{1,0:T(8,128)(2,1)} %bitcast.76, bf16[64,512]{1,0:T(8,128)(2,1)} %copy-done.4, bf16[512,2048]{1,0:T(8,128)(2,1)} %bitcast.70, ...), custom_call_target="tpu_custom_call" | custom-call | tf_op jit(solution)/shard_map/forward/pallas_call | solution.py:346
  21.7 5.4 %collective-permute-done.1.rest_1_ = bf16[1024,512]{1,0:T(8,128)(2,1)S(1)} collective-permute-done((bf16[1024,512]{1,0:T(8,128)(2,1)S(1)}, bf16[1024,512]{1,0:T(8,128)(2,1)S(1)}, u32[]{:S(2)}, u32[]{:S(2)}) %collective-permute-start.1) | collective-permute-done | bytes 1048608 | tf_op jit(solution)/shard_map/ppermute | solution.py:16
  27.0 1.0 copy-done.2
  28.1 6.8 %backward.1 = (f32[2048,128]{1,0:T(8,128)}, f32[32,512]{1,0:T(8,128)}, f32[2,512]{1,0:T(2,128)}) custom-call(bf16[512,2048]{1,0:T(8,128)(2,1)} %bitcast.71, f32[512,512]{1,0:T(8,128)} %get-tuple-element.16.normed, f32[512,128]{1,0:T(8,128)} %get-tuple-element.17.inv_in, f32[1,512]{1,0:T(1,128)} %bitcast.85, f32[1,512]{1,0:T(1,128)} %bitcast.87, ...), custom_call_target="tpu_custom_call" | custom-call | tf_op jit(solution)/shard_map/backward/pallas_call | solution.py:371
  34.9 8.2 %taps.1 = f32[40,512]{1,0:T(8,128)} custom-call(f32[2048,128]{1,0:T(8,128)} %get-tuple-element.18.grads, f32[2304,128]{1,0:T(8,128)} %get-tuple-element.24.gated, f32[2,512]{1,0:T(2,128)} %get-tuple-element.25.sums), custom_call_target="tpu_custom_call" | custom-call | tf_op jit(solution)/shard_map/taps/pallas_call | solution.py:380
  43.2 1.4 %collective-permute-done.28 = f32[40,512]{1,0:T(8,128)S(1)} collective-permute-done((f32[40,512]{1,0:T(8,128)}, f32[40,512]{1,0:T(8,128)S(1)}, u32[]{:S(2)}, u32[]{:S(2)}) %collective-permute-start.28) | collective-permute-done | bytes 81952 | tf_op jit(solution)/shard_map/ppermute | solution.py:16
  44.6 0.9 add.158
  45.5 2.4 %collective-permute-start.29 = (f32[40,512]{1,0:T(8,128)S(1)}, f32[40,512]{1,0:T(8,128)S(1)}, u32[]{:S(2)}, u32[]{:S(2)}) collective-permute-start(f32[40,512]{1,0:T(8,128)S(1)} %add.158), channel_id=1, source_target_pairs={{0,2},{2,0},{4,6},{6,4},{8,10},{10,8},{12,14},{14,12},{16,18},{18,... | collective-permute-start | bytes 245768 | tf_op jit(solution)/shard_map/ppermute | solution.py:16
  47.9 1.5 %collective-permute-start.30 = (f32[40,512]{1,0:T(8,128)S(1)}, f32[40,512]{1,0:T(8,128)S(1)}, u32[]{:S(2)}, u32[]{:S(2)}) collective-permute-start(f32[40,512]{1,0:T(8,128)S(1)} %add.158), channel_id=1, source_target_pairs={{0,4},{2,6},{4,0},{6,2},{8,12},{10,14},{12,8},{14,10},{16,20},{18,... | collective-permute-start | bytes 245768 | tf_op jit(solution)/shard_map/ppermute | solution.py:16
  49.4 0.9 collective-permute-start.31
  50.3 1.3 collective-permute-start.2
  51.7 4.7 %collective-permute-done.2.halo = f32[32,512]{1,0:T(8,128)S(1)} collective-permute-done((f32[32,512]{1,0:T(8,128)S(1)}, f32[32,512]{1,0:T(8,128)S(1)}, u32[]{:S(2)}, u32[]{:S(2)}) %collective-permute-start.2) | collective-permute-done | bytes 65568 | tf_op jit(solution)/shard_map/ppermute | solution.py:379
  57.1 7.5 %inputs.1 = (bf16[512,512]{1,0:T(8,128)(2,1)}, bf16[512,512]{1,0:T(8,128)(2,1)}) custom-call(f32[2048,128]{1,0:T(8,128)} %get-tuple-element.18.grads, f32[32,512]{1,0:T(8,128)} %copy-done.3, f32[31,512]{1,0:T(8,128)} %weight.3, bf16[512,512]{1,0:T(8,128)(2,1)} %bitcast.75, bf16[512,512]{1,0:T(8,128)(2,1)} %bitcast.77), custom_call_target="tpu_custom_call" | custom-call | tf_op jit(solution)/shard_map/inputs/pallas_call | solution.py:388
  64.7 3.0 %collective-permute-start.32 = (f32[40,512]{1,0:T(8,128)S(1)}, f32[40,512]{1,0:T(8,128)S(1)}, u32[]{:S(2)}, u32[]{:S(2)}) collective-permute-start(f32[40,512]{1,0:T(8,128)S(1)} %add_add_fusion.1), channel_id=1, source_target_pairs={{0,8},{2,10},{4,12},{6,14},{8,0},{10,2},{12,4},{14,6},{16,24},{18,... | collective-permute-start | bytes 245768 | tf_op jit(solution)/shard_map/ppermute | solution.py:16
  67.7 2.6 %collective-permute-start.33 = (f32[40,512]{1,0:T(8,128)S(1)}, f32[40,512]{1,0:T(8,128)S(1)}, u32[]{:S(2)}, u32[]{:S(2)}) collective-permute-start(f32[40,512]{1,0:T(8,128)S(1)} %add_add_fusion.1), channel_id=1, source_target_pairs={{0,16},{2,18},{4,20},{6,22},{8,24},{10,26},{12,28},{14,30},{16,0},... | collective-permute-start | bytes 245768 | tf_op jit(solution)/shard_map/ppermute | solution.py:16
  70.3 2.1 %add.137 = f32[1024,512]{1,0:T(8,128)S(1)} add(f32[1024,512]{1,0:T(8,128)S(1)} %copy-done, f32[1024,512]{1,0:T(8,128)} %collective-permute-done.3) | non-fusion elementwise | flops 524288 | bytes 6291456 | tf_op jit(solution)/shard_map/add | solution.py:73
  72.5 3.9 %collective-permute-start.16 = (bf16[64,512]{1,0:T(8,128)(2,1)S(1)}, bf16[64,512]{1,0:T(8,128)(2,1)S(1)}, u32[]{:S(2)}, u32[]{:S(2)}) collective-permute-start(bf16[64,512]{1,0:T(8,128)(2,1)S(1)} %get-tuple-element.29), channel_id=1, source_target_pairs={{0,24},{2,26},{4,28},{6,30},{8,16},{10,18},{12,20},{14,22},{16,8},... | collective-permute-start | bytes 196616 | tf_op jit(solution)/shard_map/ppermute | solution.py:16
  76.3 0.6 collective-permute-start.18
  77.6 1.5 %collective-permute-done.16 = bf16[64,512]{1,0:T(8,128)(2,1)S(1)} collective-permute-done((bf16[64,512]{1,0:T(8,128)(2,1)S(1)}, bf16[64,512]{1,0:T(8,128)(2,1)S(1)}, u32[]{:S(2)}, u32[]{:S(2)}) %collective-permute-start.16) | collective-permute-done | bytes 65568 | tf_op jit(solution)/shard_map/ppermute | solution.py:16
  79.1 3.1 %collective-permute-done.17 = bf16[64,512]{1,0:T(8,128)(2,1)S(1)} collective-permute-done((bf16[64,512]{1,0:T(8,128)(2,1)S(1)}, bf16[64,512]{1,0:T(8,128)(2,1)S(1)}, u32[]{:S(2)}, u32[]{:S(2)}) %collective-permute-start.17) | collective-permute-done | bytes 65568 | tf_op jit(solution)/shard_map/ppermute | solution.py:16
  82.2 2.1 %collective-permute-start.19 = (bf16[16,512]{1,0:T(8,128)(2,1)S(1)}, bf16[16,512]{1,0:T(8,128)(2,1)S(1)}, u32[]{:S(2)}, u32[]{:S(2)}) collective-permute-start(bf16[16,512]{1,0:T(8,128)(2,1)S(1)} %get-tuple-element.35), channel_id=1, source_target_pairs={{0,6},{2,4},{4,2},{6,0},{8,14},{10,12},{12,10},{14,8},{16,22},{18,... | collective-permute-start | bytes 49160 | tf_op jit(solution)/shard_map/ppermute | solution.py:16
  84.7 1.0 collective-permute-start.21
  86.4 0.6 slice.38
  87.1 0.9 collective-permute-done.20
  88.5 1.1 collective-permute-start.24
  89.7 2.1 %collective-permute-start.4 = (bf16[192,512]{1,0:T(8,128)(2,1)S(1)}, bf16[192,512]{1,0:T(8,128)(2,1)S(1)}, u32[]{:S(2)}, u32[]{:S(2)}) collective-permute-start(bf16[192,512]{1,0:T(8,128)(2,1)S(1)} %get-tuple-element.26), channel_id=1, source_target_pairs={{0,6},{2,4},{4,2},{6,0},{8,14},{10,12},{12,10},{14,8},{16,22},{18,... | collective-permute-start | bytes 589832 | tf_op jit(solution)/shard_map/ppermute | solution.py:16
  92.2 1.0 collective-permute-start.6
  93.2 2.0 %collective-permute-start.22 = (bf16[16,512]{1,0:T(8,128)(2,1)S(1)}, bf16[16,512]{1,0:T(8,128)(2,1)S(1)}, u32[]{:S(2)}, u32[]{:S(2)}) collective-permute-start(bf16[16,512]{1,0:T(8,128)(2,1)S(1)} %fusion.18), channel_id=1, source_target_pairs={{0,6},{2,4},{4,2},{6,0},{8,14},{10,12},{12,10},{14,8},{16,22},{18,... | collective-permute-start | bytes 49160 | tf_op jit(solution)/shard_map/ppermute | solution.py:16
  95.7 3.5 %collective-permute-done.22 = bf16[16,512]{1,0:T(8,128)(2,1)S(1)} collective-permute-done((bf16[16,512]{1,0:T(8,128)(2,1)S(1)}, bf16[16,512]{1,0:T(8,128)(2,1)S(1)}, u32[]{:S(2)}, u32[]{:S(2)}) %collective-permute-start.22) | collective-permute-done | bytes 16416 | tf_op jit(solution)/shard_map/ppermute | solution.py:16
  99.4 2.5 %collective-permute-start.7 = (bf16[48,512]{1,0:T(8,128)(2,1)S(1)}, bf16[48,512]{1,0:T(8,128)(2,1)S(1)}, u32[]{:S(2)}, u32[]{:S(2)}) collective-permute-start(bf16[48,512]{1,0:T(8,128)(2,1)S(1)} %get-tuple-element.32), channel_id=1, source_target_pairs={{0,24},{2,26},{4,28},{6,30},{8,16},{10,18},{12,20},{14,22},{16,8},... | collective-permute-start | bytes 147464 | tf_op jit(solution)/shard_map/ppermute | solution.py:16
  101.8 2.0 %collective-permute-start.9 = (bf16[48,512]{1,0:T(8,128)(2,1)S(1)}, bf16[48,512]{1,0:T(8,128)(2,1)S(1)}, u32[]{:S(2)}, u32[]{:S(2)}) collective-permute-start(bf16[48,512]{1,0:T(8,128)(2,1)S(1)} %get-tuple-element.33), channel_id=1, source_target_pairs={{0,8},{2,10},{4,12},{6,14},{8,0},{10,2},{12,4},{14,6},{16,24},{18,... | collective-permute-start | bytes 147464 | tf_op jit(solution)/shard_map/ppermute | solution.py:16
  103.8 2.5 %collective-permute-start.25 = (bf16[64,512]{1,0:T(8,128)(2,1)S(1)}, bf16[64,512]{1,0:T(8,128)(2,1)S(1)}, u32[]{:S(2)}, u32[]{:S(2)}) collective-permute-start(bf16[64,512]{1,0:T(8,128)(2,1)S(1)} %maximum_select_fusion.9), channel_id=1, source_target_pairs={{0,24},{2,26},{4,28},{6,30},{8,16},{10,18},{12,20},{14,22},{16,8},... | collective-permute-start | bytes 196616 | tf_op jit(solution)/shard_map/ppermute | solution.py:16
  106.3 2.0 %collective-permute-start.27 = (bf16[64,512]{1,0:T(8,128)(2,1)S(1)}, bf16[64,512]{1,0:T(8,128)(2,1)S(1)}, u32[]{:S(2)}, u32[]{:S(2)}) collective-permute-start(bf16[64,512]{1,0:T(8,128)(2,1)S(1)} %maximum_select_fusion.9), channel_id=1, source_target_pairs={{0,8},{2,10},{4,12},{6,14},{8,0},{10,2},{12,4},{14,6},{16,24},{18,... | collective-permute-start | bytes 196616 | tf_op jit(solution)/shard_map/ppermute | solution.py:16
  108.6 2.6 %collective-permute-done.27 = bf16[64,512]{1,0:T(8,128)(2,1)S(1)} collective-permute-done((bf16[64,512]{1,0:T(8,128)(2,1)S(1)}, bf16[64,512]{1,0:T(8,128)(2,1)S(1)}, u32[]{:S(2)}, u32[]{:S(2)}) %collective-permute-start.27) | collective-permute-done | bytes 65568 | tf_op jit(solution)/shard_map/ppermute | solution.py:16
  111.3 2.1 %collective-permute-start.10 = (bf16[48,512]{1,0:T(8,128)(2,1)S(1)}, bf16[48,512]{1,0:T(8,128)(2,1)S(1)}, u32[]{:S(2)}, u32[]{:S(2)}) collective-permute-start(bf16[48,512]{1,0:T(8,128)(2,1)S(1)} %fusion.9), channel_id=1, source_target_pairs={{0,24},{2,26},{4,28},{6,30},{8,16},{10,18},{12,20},{14,22},{16,8},... | collective-permute-start | bytes 147464 | tf_op jit(solution)/shard_map/ppermute | solution.py:16
  113.3 1.2 collective-permute-start.11
  114.6 2.6 %collective-permute-done.10 = bf16[48,512]{1,0:T(8,128)(2,1)S(1)} collective-permute-done((bf16[48,512]{1,0:T(8,128)(2,1)S(1)}, bf16[48,512]{1,0:T(8,128)(2,1)S(1)}, u32[]{:S(2)}, u32[]{:S(2)}) %collective-permute-start.10) | collective-permute-done | bytes 49184 | tf_op jit(solution)/shard_map/ppermute | solution.py:16
  117.2 1.6 %collective-permute-done.11 = bf16[48,512]{1,0:T(8,128)(2,1)S(1)} collective-permute-done((bf16[48,512]{1,0:T(8,128)(2,1)S(1)}, bf16[48,512]{1,0:T(8,128)(2,1)S(1)}, u32[]{:S(2)}, u32[]{:S(2)}) %collective-permute-start.11) | collective-permute-done | bytes 49184 | tf_op jit(solution)/shard_map/ppermute | solution.py:16
  118.9 1.2 collective-permute-start.15
  120.2 1.3 collective-permute-start.13
  121.4 1.2 collective-permute-start.14
  122.6 2.0 %collective-permute-done.15 = bf16[192,512]{1,0:T(8,128)(2,1)S(1)} collective-permute-done((bf16[192,512]{1,0:T(8,128)(2,1)S(1)}, bf16[192,512]{1,0:T(8,128)(2,1)S(1)}, u32[]{:S(2)}, u32[]{:S(2)}) %collective-permute-start.15) | collective-permute-done | bytes 196640 | tf_op jit(solution)/shard_map/ppermute | solution.py:16
  124.8 2.4 %collective-permute-done.13 = bf16[192,512]{1,0:T(8,128)(2,1)S(1)} collective-permute-done((bf16[192,512]{1,0:T(8,128)(2,1)S(1)}, bf16[192,512]{1,0:T(8,128)(2,1)S(1)}, u32[]{:S(2)}, u32[]{:S(2)}) %collective-permute-start.13) | collective-permute-done | bytes 196640 | tf_op jit(solution)/shard_map/ppermute | solution.py:16
  127.2 2.0 %collective-permute-done.14 = bf16[192,512]{1,0:T(8,128)(2,1)S(1)} collective-permute-done((bf16[192,512]{1,0:T(8,128)(2,1)S(1)}, bf16[192,512]{1,0:T(8,128)(2,1)S(1)}, u32[]{:S(2)}, u32[]{:S(2)}) %collective-permute-start.14) | collective-permute-done | bytes 196640 | tf_op jit(solution)/shard_map/ppermute | solution.py:16
  129.6 1.6 %maximum_convert_fusion = f32[1024,512]{1,0:T(8,128)} fusion(bf16[256,512]{1,0:T(8,128)(2,1)S(1)} %maximum_select_fusion.3, bf16[768,512]{1,0:T(8,128)(2,1)S(1)} %maximum_select_fusion), kind=kLoop, calls=%fused_computation | loop fusion | flops 2097152 | bytes 3145728 | tf_op jit(solution)/shard_map/convert_element_type | solution.py:416
  (69 shorter events, 6.6 us)
Async XLA Ops:
  0.6 20.5 %copy-start.1 = (bf16[1024,512]{1,0:T(8,128)(2,1)S(1)}, bf16[1024,512]{1,0:T(8,128)(2,1)}, u32[]{:S(2)}) copy-start(bf16[1024,512]{1,0:T(8,128)(2,1)} %rest_0_.1) | copy-start | bytes 3145732
  1.5 6.8 %collective-permute-start = (bf16[64,512]{1,0:T(8,128)(2,1)S(1)}, bf16[64,512]{1,0:T(8,128)(2,1)S(1)}, u32[]{:S(2)}, u32[]{:S(2)}) collective-permute-start(bf16[64,512]{1,0:T(8,128)(2,1)S(1)} %pad_maximum_fusion), channel_id=1, source_target_pairs={{0,2},{2,4},{4,6},{6,8},{8,10},{10,12},{12,14},{14,16},{16,18},{18... | collective-permute-start | bytes 196616 | tf_op jit(solution)/shard_map/ppermute | solution.py:339
  8.3 0.6 copy-start.4
  21.1 49.2 %collective-permute-start.3 = (f32[1024,512]{1,0:T(8,128)}, f32[1024,512]{1,0:T(8,128)}, u32[]{:S(2)}, u32[]{:S(2)}) collective-permute-start(f32[1024,512]{1,0:T(8,128)} %bitcast.90), channel_id=1, source_target_pairs={{0,1},{1,0},{2,3},{3,2},{4,5},{5,4},{6,7},{7,6},{8,9},{9,8},{10,11... | collective-permute-start | bytes 6291464 | tf_op jit(solution)/shard_map/ppermute | solution.py:16
  21.2 5.8 %collective-permute-start.1 = (bf16[1024,512]{1,0:T(8,128)(2,1)S(1)}, bf16[1024,512]{1,0:T(8,128)(2,1)S(1)}, u32[]{:S(2)}, u32[]{:S(2)}) collective-permute-start(bf16[1024,512]{1,0:T(8,128)(2,1)S(1)} %copy-done.1), channel_id=1, source_target_pairs={{0,1},{1,0},{2,3},{3,2},{4,5},{5,4},{6,7},{7,6},{8,9},{9,8},{10,11... | collective-permute-start | bytes 3145736 | tf_op jit(solution)/shard_map/ppermute | solution.py:16
  27.0 1.0 copy-start.2
  34.9 15.4 %copy-start.5 = (f32[32,512]{1,0:T(8,128)S(1)}, f32[32,512]{1,0:T(8,128)}, u32[]{:S(2)}) copy-start(f32[32,512]{1,0:T(8,128)} %get-tuple-element.19) | copy-start | bytes 196612
  43.1 27.2 %copy-start = (f32[1024,512]{1,0:T(8,128)S(1)}, f32[1024,512]{1,0:T(8,128)}, u32[]{:S(2)}) copy-start(f32[1024,512]{1,0:T(8,128)} %get-tuple-element.22) | copy-start | bytes 6291460
  43.1 1.5 %collective-permute-start.28 = (f32[40,512]{1,0:T(8,128)}, f32[40,512]{1,0:T(8,128)S(1)}, u32[]{:S(2)}, u32[]{:S(2)}) collective-permute-start(f32[40,512]{1,0:T(8,128)} %taps.1), channel_id=1, source_target_pairs={{0,1},{1,0},{2,3},{3,2},{4,5},{5,4},{6,7},{7,6},{8,9},{9,8},{10,11... | collective-permute-start | bytes 245768 | tf_op jit(solution)/shard_map/ppermute | solution.py:16
  45.5 19.1 %collective-permute-start.29 = (f32[40,512]{1,0:T(8,128)S(1)}, f32[40,512]{1,0:T(8,128)S(1)}, u32[]{:S(2)}, u32[]{:S(2)}) collective-permute-start(f32[40,512]{1,0:T(8,128)S(1)} %add.158), channel_id=1, source_target_pairs={{0,2},{2,0},{4,6},{6,4},{8,10},{10,8},{12,14},{14,12},{16,18},{18,... | collective-permute-start | bytes 245768 | tf_op jit(solution)/shard_map/ppermute | solution.py:16
  47.9 16.7 %collective-permute-start.30 = (f32[40,512]{1,0:T(8,128)S(1)}, f32[40,512]{1,0:T(8,128)S(1)}, u32[]{:S(2)}, u32[]{:S(2)}) collective-permute-start(f32[40,512]{1,0:T(8,128)S(1)} %add.158), channel_id=1, source_target_pairs={{0,4},{2,6},{4,0},{6,2},{8,12},{10,14},{12,8},{14,10},{16,20},{18,... | collective-permute-start | bytes 245768 | tf_op jit(solution)/shard_map/ppermute | solution.py:16
  49.4 15.2 %collective-permute-start.31 = (f32[40,512]{1,0:T(8,128)S(1)}, f32[40,512]{1,0:T(8,128)S(1)}, u32[]{:S(2)}, u32[]{:S(2)}) collective-permute-start(f32[40,512]{1,0:T(8,128)S(1)} %add.158), channel_id=1, source_target_pairs={{0,6},{2,4},{4,2},{6,0},{8,14},{10,12},{12,10},{14,8},{16,22},{18,... | collective-permute-start | bytes 245768 | tf_op jit(solution)/shard_map/ppermute | solution.py:16
  50.3 6.1 %collective-permute-start.2 = (f32[32,512]{1,0:T(8,128)S(1)}, f32[32,512]{1,0:T(8,128)S(1)}, u32[]{:S(2)}, u32[]{:S(2)}) collective-permute-start(f32[32,512]{1,0:T(8,128)S(1)} %copy-done.5), channel_id=1, source_target_pairs={{2,0},{4,2},{6,4},{8,6},{10,8},{12,10},{14,12},{16,14},{18,16},{20... | collective-permute-start | bytes 196616 | tf_op jit(solution)/shard_map/ppermute | solution.py:379
  56.4 0.6 copy-start.3
  64.7 11.7 %collective-permute-start.32 = (f32[40,512]{1,0:T(8,128)S(1)}, f32[40,512]{1,0:T(8,128)S(1)}, u32[]{:S(2)}, u32[]{:S(2)}) collective-permute-start(f32[40,512]{1,0:T(8,128)S(1)} %add_add_fusion.1), channel_id=1, source_target_pairs={{0,8},{2,10},{4,12},{6,14},{8,0},{10,2},{12,4},{14,6},{16,24},{18,... | collective-permute-start | bytes 245768 | tf_op jit(solution)/shard_map/ppermute | solution.py:16
  67.7 9.9 %collective-permute-start.33 = (f32[40,512]{1,0:T(8,128)S(1)}, f32[40,512]{1,0:T(8,128)S(1)}, u32[]{:S(2)}, u32[]{:S(2)}) collective-permute-start(f32[40,512]{1,0:T(8,128)S(1)} %add_add_fusion.1), channel_id=1, source_target_pairs={{0,16},{2,18},{4,20},{6,22},{8,24},{10,26},{12,28},{14,30},{16,0},... | collective-permute-start | bytes 245768 | tf_op jit(solution)/shard_map/ppermute | solution.py:16
  70.3 7.3 %collective-permute-start.34 = (f32[40,512]{1,0:T(8,128)S(1)}, f32[40,512]{1,0:T(8,128)S(1)}, u32[]{:S(2)}, u32[]{:S(2)}) collective-permute-start(f32[40,512]{1,0:T(8,128)S(1)} %add_add_fusion.1), channel_id=1, source_target_pairs={{0,24},{2,26},{4,28},{6,30},{8,16},{10,18},{12,20},{14,22},{16,8},... | collective-permute-start | bytes 245768 | tf_op jit(solution)/shard_map/ppermute | solution.py:16
  72.5 6.7 %collective-permute-start.16 = (bf16[64,512]{1,0:T(8,128)(2,1)S(1)}, bf16[64,512]{1,0:T(8,128)(2,1)S(1)}, u32[]{:S(2)}, u32[]{:S(2)}) collective-permute-start(bf16[64,512]{1,0:T(8,128)(2,1)S(1)} %get-tuple-element.29), channel_id=1, source_target_pairs={{0,24},{2,26},{4,28},{6,30},{8,16},{10,18},{12,20},{14,22},{16,8},... | collective-permute-start | bytes 196616 | tf_op jit(solution)/shard_map/ppermute | solution.py:16
  76.3 5.8 %collective-permute-start.17 = (bf16[64,512]{1,0:T(8,128)(2,1)S(1)}, bf16[64,512]{1,0:T(8,128)(2,1)S(1)}, u32[]{:S(2)}, u32[]{:S(2)}) collective-permute-start(bf16[64,512]{1,0:T(8,128)(2,1)S(1)} %get-tuple-element.31), channel_id=1, source_target_pairs={{0,16},{2,18},{4,20},{6,22},{8,24},{10,26},{12,28},{14,30},{16,0},... | collective-permute-start | bytes 196616 | tf_op jit(solution)/shard_map/ppermute | solution.py:16
  76.3 5.8 %collective-permute-start.18 = (bf16[64,512]{1,0:T(8,128)(2,1)S(1)}, bf16[64,512]{1,0:T(8,128)(2,1)S(1)}, u32[]{:S(2)}, u32[]{:S(2)}) collective-permute-start(bf16[64,512]{1,0:T(8,128)(2,1)S(1)} %get-tuple-element.30), channel_id=1, source_target_pairs={{0,8},{2,10},{4,12},{6,14},{8,0},{10,2},{12,4},{14,6},{16,24},{18,... | collective-permute-start | bytes 196616 | tf_op jit(solution)/shard_map/ppermute | solution.py:16
  82.2 4.9 %collective-permute-start.19 = (bf16[16,512]{1,0:T(8,128)(2,1)S(1)}, bf16[16,512]{1,0:T(8,128)(2,1)S(1)}, u32[]{:S(2)}, u32[]{:S(2)}) collective-permute-start(bf16[16,512]{1,0:T(8,128)(2,1)S(1)} %get-tuple-element.35), channel_id=1, source_target_pairs={{0,6},{2,4},{4,2},{6,0},{8,14},{10,12},{12,10},{14,8},{16,22},{18,... | collective-permute-start | bytes 49160 | tf_op jit(solution)/shard_map/ppermute | solution.py:16
  84.3 3.7 %collective-permute-start.20 = (bf16[16,512]{1,0:T(8,128)(2,1)S(1)}, bf16[16,512]{1,0:T(8,128)(2,1)S(1)}, u32[]{:S(2)}, u32[]{:S(2)}) collective-permute-start(bf16[16,512]{1,0:T(8,128)(2,1)S(1)} %get-tuple-element.37), channel_id=1, source_target_pairs={{0,4},{2,6},{4,0},{6,2},{8,12},{10,14},{12,8},{14,10},{16,20},{18,... | collective-permute-start | bytes 49160 | tf_op jit(solution)/shard_map/ppermute | solution.py:16
  84.7 3.7 %collective-permute-start.21 = (bf16[16,512]{1,0:T(8,128)(2,1)S(1)}, bf16[16,512]{1,0:T(8,128)(2,1)S(1)}, u32[]{:S(2)}, u32[]{:S(2)}) collective-permute-start(bf16[16,512]{1,0:T(8,128)(2,1)S(1)} %get-tuple-element.36), channel_id=1, source_target_pairs={{0,2},{2,0},{4,6},{6,4},{8,10},{10,8},{12,14},{14,12},{16,18},{18,... | collective-permute-start | bytes 49160 | tf_op jit(solution)/shard_map/ppermute | solution.py:16
  88.5 6.7 %collective-permute-start.24 = (bf16[16,512]{1,0:T(8,128)(2,1)S(1)}, bf16[16,512]{1,0:T(8,128)(2,1)S(1)}, u32[]{:S(2)}, u32[]{:S(2)}) collective-permute-start(bf16[16,512]{1,0:T(8,128)(2,1)S(1)} %fusion.18), channel_id=1, source_target_pairs={{0,2},{2,0},{4,6},{6,4},{8,10},{10,8},{12,14},{14,12},{16,18},{18,... | collective-permute-start | bytes 49160 | tf_op jit(solution)/shard_map/ppermute | solution.py:16
  89.7 9.5 %collective-permute-start.4 = (bf16[192,512]{1,0:T(8,128)(2,1)S(1)}, bf16[192,512]{1,0:T(8,128)(2,1)S(1)}, u32[]{:S(2)}, u32[]{:S(2)}) collective-permute-start(bf16[192,512]{1,0:T(8,128)(2,1)S(1)} %get-tuple-element.26), channel_id=1, source_target_pairs={{0,6},{2,4},{4,2},{6,0},{8,14},{10,12},{12,10},{14,8},{16,22},{18,... | collective-permute-start | bytes 589832 | tf_op jit(solution)/shard_map/ppermute | solution.py:16
  91.7 7.4 %collective-permute-start.5 = (bf16[192,512]{1,0:T(8,128)(2,1)S(1)}, bf16[192,512]{1,0:T(8,128)(2,1)S(1)}, u32[]{:S(2)}, u32[]{:S(2)}) collective-permute-start(bf16[192,512]{1,0:T(8,128)(2,1)S(1)} %get-tuple-element.28), channel_id=1, source_target_pairs={{0,4},{2,6},{4,0},{6,2},{8,12},{10,14},{12,8},{14,10},{16,20},{18,... | collective-permute-start | bytes 589832 | tf_op jit(solution)/shard_map/ppermute | solution.py:16
  92.2 7.0 %collective-permute-start.6 = (bf16[192,512]{1,0:T(8,128)(2,1)S(1)}, bf16[192,512]{1,0:T(8,128)(2,1)S(1)}, u32[]{:S(2)}, u32[]{:S(2)}) collective-permute-start(bf16[192,512]{1,0:T(8,128)(2,1)S(1)} %get-tuple-element.27), channel_id=1, source_target_pairs={{0,2},{2,0},{4,6},{6,4},{8,10},{10,8},{12,14},{14,12},{16,18},{18,... | collective-permute-start | bytes 589832 | tf_op jit(solution)/shard_map/ppermute | solution.py:16
  93.2 5.9 %collective-permute-start.22 = (bf16[16,512]{1,0:T(8,128)(2,1)S(1)}, bf16[16,512]{1,0:T(8,128)(2,1)S(1)}, u32[]{:S(2)}, u32[]{:S(2)}) collective-permute-start(bf16[16,512]{1,0:T(8,128)(2,1)S(1)} %fusion.18), channel_id=1, source_target_pairs={{0,6},{2,4},{4,2},{6,0},{8,14},{10,12},{12,10},{14,8},{16,22},{18,... | collective-permute-start | bytes 49160 | tf_op jit(solution)/shard_map/ppermute | solution.py:16
  95.2 3.9 %collective-permute-start.23 = (bf16[16,512]{1,0:T(8,128)(2,1)S(1)}, bf16[16,512]{1,0:T(8,128)(2,1)S(1)}, u32[]{:S(2)}, u32[]{:S(2)}) collective-permute-start(bf16[16,512]{1,0:T(8,128)(2,1)S(1)} %fusion.18), channel_id=1, source_target_pairs={{0,4},{2,6},{4,0},{6,2},{8,12},{10,14},{12,8},{14,10},{16,20},{18,... | collective-permute-start | bytes 49160 | tf_op jit(solution)/shard_map/ppermute | solution.py:16
  99.4 6.9 %collective-permute-start.7 = (bf16[48,512]{1,0:T(8,128)(2,1)S(1)}, bf16[48,512]{1,0:T(8,128)(2,1)S(1)}, u32[]{:S(2)}, u32[]{:S(2)}) collective-permute-start(bf16[48,512]{1,0:T(8,128)(2,1)S(1)} %get-tuple-element.32), channel_id=1, source_target_pairs={{0,24},{2,26},{4,28},{6,30},{8,16},{10,18},{12,20},{14,22},{16,8},... | collective-permute-start | bytes 147464 | tf_op jit(solution)/shard_map/ppermute | solution.py:16
  101.8 6.5 %collective-permute-start.8 = (bf16[48,512]{1,0:T(8,128)(2,1)S(1)}, bf16[48,512]{1,0:T(8,128)(2,1)S(1)}, u32[]{:S(2)}, u32[]{:S(2)}) collective-permute-start(bf16[48,512]{1,0:T(8,128)(2,1)S(1)} %get-tuple-element.34), channel_id=1, source_target_pairs={{0,16},{2,18},{4,20},{6,22},{8,24},{10,26},{12,28},{14,30},{16,0},... | collective-permute-start | bytes 147464 | tf_op jit(solution)/shard_map/ppermute | solution.py:16
  101.8 6.5 %collective-permute-start.9 = (bf16[48,512]{1,0:T(8,128)(2,1)S(1)}, bf16[48,512]{1,0:T(8,128)(2,1)S(1)}, u32[]{:S(2)}, u32[]{:S(2)}) collective-permute-start(bf16[48,512]{1,0:T(8,128)(2,1)S(1)} %get-tuple-element.33), channel_id=1, source_target_pairs={{0,8},{2,10},{4,12},{6,14},{8,0},{10,2},{12,4},{14,6},{16,24},{18,... | collective-permute-start | bytes 147464 | tf_op jit(solution)/shard_map/ppermute | solution.py:16
  103.8 16.3 %collective-permute-start.25 = (bf16[64,512]{1,0:T(8,128)(2,1)S(1)}, bf16[64,512]{1,0:T(8,128)(2,1)S(1)}, u32[]{:S(2)}, u32[]{:S(2)}) collective-permute-start(bf16[64,512]{1,0:T(8,128)(2,1)S(1)} %maximum_select_fusion.9), channel_id=1, source_target_pairs={{0,24},{2,26},{4,28},{6,30},{8,16},{10,18},{12,20},{14,22},{16,8},... | collective-permute-start | bytes 196616 | tf_op jit(solution)/shard_map/ppermute | solution.py:16
  106.3 13.8 %collective-permute-start.26 = (bf16[64,512]{1,0:T(8,128)(2,1)S(1)}, bf16[64,512]{1,0:T(8,128)(2,1)S(1)}, u32[]{:S(2)}, u32[]{:S(2)}) collective-permute-start(bf16[64,512]{1,0:T(8,128)(2,1)S(1)} %maximum_select_fusion.9), channel_id=1, source_target_pairs={{0,16},{2,18},{4,20},{6,22},{8,24},{10,26},{12,28},{14,30},{16,0},... | collective-permute-start | bytes 196616 | tf_op jit(solution)/shard_map/ppermute | solution.py:16
  106.3 4.9 %collective-permute-start.27 = (bf16[64,512]{1,0:T(8,128)(2,1)S(1)}, bf16[64,512]{1,0:T(8,128)(2,1)S(1)}, u32[]{:S(2)}, u32[]{:S(2)}) collective-permute-start(bf16[64,512]{1,0:T(8,128)(2,1)S(1)} %maximum_select_fusion.9), channel_id=1, source_target_pairs={{0,8},{2,10},{4,12},{6,14},{8,0},{10,2},{12,4},{14,6},{16,24},{18,... | collective-permute-start | bytes 196616 | tf_op jit(solution)/shard_map/ppermute | solution.py:16
  108.3 6.3 %collective-permute-start.12 = (bf16[48,512]{1,0:T(8,128)(2,1)S(1)}, bf16[48,512]{1,0:T(8,128)(2,1)S(1)}, u32[]{:S(2)}, u32[]{:S(2)}) collective-permute-start(bf16[48,512]{1,0:T(8,128)(2,1)S(1)} %fusion.9), channel_id=1, source_target_pairs={{0,8},{2,10},{4,12},{6,14},{8,0},{10,2},{12,4},{14,6},{16,24},{18,... | collective-permute-start | bytes 147464 | tf_op jit(solution)/shard_map/ppermute | solution.py:16
  111.3 6.0 %collective-permute-start.10 = (bf16[48,512]{1,0:T(8,128)(2,1)S(1)}, bf16[48,512]{1,0:T(8,128)(2,1)S(1)}, u32[]{:S(2)}, u32[]{:S(2)}) collective-permute-start(bf16[48,512]{1,0:T(8,128)(2,1)S(1)} %fusion.9), channel_id=1, source_target_pairs={{0,24},{2,26},{4,28},{6,30},{8,16},{10,18},{12,20},{14,22},{16,8},... | collective-permute-start | bytes 147464 | tf_op jit(solution)/shard_map/ppermute | solution.py:16
  113.3 5.5 %collective-permute-start.11 = (bf16[48,512]{1,0:T(8,128)(2,1)S(1)}, bf16[48,512]{1,0:T(8,128)(2,1)S(1)}, u32[]{:S(2)}, u32[]{:S(2)}) collective-permute-start(bf16[48,512]{1,0:T(8,128)(2,1)S(1)} %fusion.9), channel_id=1, source_target_pairs={{0,16},{2,18},{4,20},{6,22},{8,24},{10,26},{12,28},{14,30},{16,0},... | collective-permute-start | bytes 147464 | tf_op jit(solution)/shard_map/ppermute | solution.py:16
  118.9 5.7 %collective-permute-start.15 = (bf16[192,512]{1,0:T(8,128)(2,1)S(1)}, bf16[192,512]{1,0:T(8,128)(2,1)S(1)}, u32[]{:S(2)}, u32[]{:S(2)}) collective-permute-start(bf16[192,512]{1,0:T(8,128)(2,1)S(1)} %maximum_select_fusion.4), channel_id=1, source_target_pairs={{0,2},{2,0},{4,6},{6,4},{8,10},{10,8},{12,14},{14,12},{16,18},{18,... | collective-permute-start | bytes 589832 | tf_op jit(solution)/shard_map/ppermute | solution.py:16
  120.2 7.0 %collective-permute-start.13 = (bf16[192,512]{1,0:T(8,128)(2,1)S(1)}, bf16[192,512]{1,0:T(8,128)(2,1)S(1)}, u32[]{:S(2)}, u32[]{:S(2)}) collective-permute-start(bf16[192,512]{1,0:T(8,128)(2,1)S(1)} %maximum_select_fusion.4), channel_id=1, source_target_pairs={{0,6},{2,4},{4,2},{6,0},{8,14},{10,12},{12,10},{14,8},{16,22},{18,... | collective-permute-start | bytes 589832 | tf_op jit(solution)/shard_map/ppermute | solution.py:16
  121.4 7.8 %collective-permute-start.14 = (bf16[192,512]{1,0:T(8,128)(2,1)S(1)}, bf16[192,512]{1,0:T(8,128)(2,1)S(1)}, u32[]{:S(2)}, u32[]{:S(2)}) collective-permute-start(bf16[192,512]{1,0:T(8,128)(2,1)S(1)} %maximum_select_fusion.4), channel_id=1, source_target_pairs={{0,4},{2,6},{4,0},{6,2},{8,12},{10,14},{12,8},{14,10},{16,20},{18,... | collective-permute-start | bytes 589832 | tf_op jit(solution)/shard_map/ppermute | solution.py:16

commit v3 on v2

v3 whole, which is shorter than its diff:
```python
import functools
import math

import jax
import jax.numpy as jnp
from jax import lax
from jax.experimental import pallas as pl
from jax.experimental.pallas import tpu as pltpu
from jax.sharding import PartitionSpec as P

epsilon = 1e-06


def exchange(value, offset_of):
    count_sp = lax.axis_size("sp")
    count_dp = lax.axis_size("dp")
    pairs = []
    for d in range(count_dp):
        over_sp, over_dp = offset_of(d)
        for s in range(count_sp):
            pairs.append((s * count_dp + d, (s ^ over_sp) * count_dp + (d ^ over_dp)))
    return lax.ppermute(value, ("sp", "dp"), pairs)


def levels_of(count_sp, turn):
    bits = count_sp.bit_length() - 1
    levels = [(1 << low, 1 << min(2, bits - low)) for low in range(0, bits, 2)]
    if len({width for _, width in levels}) > 1:
        return levels
    turn %= max(len(levels), 1)
    return levels[turn:] + levels[:turn]


def digit(step):
    low = jnp.int32(1)
    for d in range(lax.axis_size("dp")):
        mine = levels_of(lax.axis_size("sp"), d)[step][0]
        low = jnp.where(lax.axis_index("dp") == d, mine, low)
    return (lax.axis_index("sp") // low) % width_of(step)


def width_of(step):
    return levels_of(lax.axis_size("sp"), 0)[step][1]


def exchange_digit(value, step, other):
    count_sp = lax.axis_size("sp")
    return exchange(value, lambda d: (levels_of(count_sp, d)[step][0] * other, 0))


def row_block(value, index, count):
    rows = value.shape[0] // count
    return lax.dynamic_slice_in_dim(value, index * rows, rows, 0)


def reduce_level(total, step, kind):
    width = width_of(step)
    mine = digit(step)
    arrived = [
        exchange_digit(row_block(total, mine ^ other, width).astype(kind), step, other)
        for other in range(width - 1, 0, -1)
    ]
    kept = row_block(total, mine, width)
    for part in arrived:
        kept = kept + part.astype(jnp.float32)
    return kept


def tree(items):
    while len(items) > 1:
        items = [items[i] + items[i + 1] for i in range(0, len(items), 2)]
    return items[0]


def two_halves(value):
    first = value.astype(jnp.bfloat16)
    return jnp.concatenate([first, (value - first.astype(jnp.float32)).astype(jnp.bfloat16)], axis=0)


def gather_level(rows, small, step):
    width = width_of(step)
    mine = digit(step)
    count = rows.shape[0]
    both = jnp.concatenate([rows, two_halves(small)], axis=0)
    pieces = [both] + [None] * (width - 1)
    for other in range(width - 1, 0, -1):
        pieces[other] = exchange_digit(both, step, other)
    half = small.shape[0]
    small = tree(
        [
            p[count : count + half].astype(jnp.float32) + p[count + half :].astype(jnp.float32)
            for p in pieces
        ]
    )
    pieces = [p[:count] for p in pieces]
    bit = 1
    while bit < width:
        swap = (mine // bit) % 2 == 1
        pieces = [
            jnp.where(
                swap,
                jnp.concatenate([pieces[i + 1], pieces[i]], axis=0),
                jnp.concatenate([pieces[i], pieces[i + 1]], axis=0),
            )
            for i in range(0, len(pieces), 2)
        ]
        bit *= 2
    return pieces[0], small


lanes = 128
sublanes = 8


def rounded_up(count, unit):
    return -(-count // unit) * unit


def strided(first, count):
    return pl.ds(first, count, stride=sublanes)


def tile(row):
    return pl.ds(pl.multiple_of(row * sublanes, sublanes), sublanes)


def grad_weight(out, cotan, act, block, scale):
    features = out.shape[0]
    step = min(features, 256)
    for f in range(0, features, step):
        at = pl.multiple_of(block * features + f, lanes)
        part = lax.dot_general(
            cotan[:, pl.ds(at, step)],
            act[...],
            (((0,), (0,)), ((), ())),
            preferred_element_type=jnp.float32,
        )
        out[f : f + step, :] = (part * scale).astype(out.dtype)


def fwd_kernel(value, gate, halo, cotan, weight, gain, shift, *rest, taps, pad, seg, eps, scale, others):
    sent = rest[:others]
    act, gated, normed, inv_out, taps_in, conv = rest[others:]
    length, channels = value.shape
    groups = channels // lanes
    segments = length // seg

    def gate_rows(v, g):
        return v.astype(jnp.float32) * jax.nn.sigmoid(g.astype(jnp.float32))

    for k in range(groups):
        cols = slice(k * lanes, (k + 1) * lanes)
        gated[strided(k, pad), :] = gate_rows(halo[:pad, cols], halo[pad:, cols])
        for s in range(segments):
            b = s * groups + k
            block = gate_rows(value[s * seg : (s + 1) * seg, cols], gate[s * seg : (s + 1) * seg, cols])
            gated[strided(pad * sublanes + b, seg), :] = block
            if s + 1 < segments:
                gated[strided(b + groups, pad), :] = block[seg - pad :]
            taps_in[strided(b, taps), :] = weight[:, cols]
    tap = [taps_in[tile(j), :] for j in range(taps)]
    unit = 16

    def conv_block(i, carry):
        base = i * unit
        sums = [None] * unit
        for m in range(unit + taps - 1):
            row = gated[tile(base + (pad - taps + 1) + m), :]
            for u in range(unit):
                j = m - u
                if 0 <= j < taps:
                    term = tap[j] * row
                    sums[u] = term if sums[u] is None else sums[u] + term
        for u in range(unit):
            conv[tile(base + u), :] = sums[u]
        return carry

    lax.fori_loop(0, seg // unit, conv_block, 0)
    chunk = 128
    for s in range(segments):

        def norm_block(i, carry, s=s):
            base = pl.multiple_of(i * chunk, chunk)
            out = pl.multiple_of(s * seg + i * chunk, chunk)
            parts = [
                conv[strided(base * sublanes + s * groups + k, chunk), :] for k in range(groups)
            ]
            mean = jnp.sum(sum(parts), axis=-1, keepdims=True) / channels
            parts = [p - mean for p in parts]
            var = jnp.sum(sum(p * p for p in parts), axis=-1, keepdims=True) / channels
            inv = lax.rsqrt(var + eps)
            inv_out[pl.ds(out, chunk), :] = jnp.broadcast_to(inv, (chunk, lanes))
            for k in range(groups):
                cols = slice(k * lanes, (k + 1) * lanes)
                n = parts[k] * inv
                normed[pl.ds(out, chunk), cols] = n
                pre = n * gain[:, cols] + shift[:, cols]
                act[pl.ds(out, chunk), cols] = (pre * jax.nn.sigmoid(pre)).astype(jnp.bfloat16)
            return carry

        lax.fori_loop(0, seg // chunk, norm_block, 0)
    for other in range(1, others + 1):
        grad_weight(sent[other - 1], cotan, act, lax.axis_index("dp") ^ other, scale)


def bwd_kernel(cotan, act, normed, inv_in, gain, shift, *rest, seg, scale, pieces):
    weights = rest[:pieces]
    own, grads, head, sums, grad_act = rest[pieces:]
    length, channels = normed.shape
    groups = channels // lanes
    segments = length // seg
    features = weights[0].shape[0]
    index = lax.axis_index("dp")
    grad_weight(own, cotan, act, index, scale)
    for other in range(pieces):
        at = pl.multiple_of((index ^ other) * features, lanes)
        part = jnp.dot(
            cotan[:, pl.ds(at, features)], weights[other][...], preferred_element_type=jnp.float32
        )
        grad_act[...] = part if other == 0 else grad_act[...] + part
    chunk = 128
    total = tuple(jnp.zeros((sublanes, lanes), jnp.float32) for _ in range(2 * groups))
    for s in range(segments):

        def grad_block(i, carry, s=s):
            base = pl.multiple_of(i * chunk, chunk)
            at = pl.multiple_of(s * seg + i * chunk, chunk)
            inv = inv_in[pl.ds(at, chunk), :]
            carry = list(carry)
            n, gn = [], []
            for k in range(groups):
                cols = slice(k * lanes, (k + 1) * lanes)
                nk = normed[pl.ds(at, chunk), cols]
                pre = nk * gain[:, cols] + shift[:, cols]
                sig = jax.nn.sigmoid(pre)
                grad_pre = grad_act[pl.ds(at, chunk), cols] * sig * (1.0 + pre * (1.0 - sig))
                by_gain = (grad_pre * nk).reshape(chunk // sublanes, sublanes, lanes)
                by_shift = grad_pre.reshape(chunk // sublanes, sublanes, lanes)
                carry[k] = carry[k] + jnp.sum(by_gain, axis=0)
                carry[groups + k] = carry[groups + k] + jnp.sum(by_shift, axis=0)
                n.append(nk)
                gn.append(grad_pre * gain[:, cols])
            mean = jnp.sum(sum(gn), axis=-1, keepdims=True) / channels
            slope = jnp.sum(sum(a * b for a, b in zip(gn, n)), axis=-1, keepdims=True) / channels
            for k in range(groups):
                grads[strided(base * sublanes + s * groups + k, chunk), :] = inv * (
                    gn[k] - mean - n[k] * slope
                )
            return tuple(carry)

        total = lax.fori_loop(0, seg // chunk, grad_block, total)
    pad = head.shape[0]
    for k in range(groups):
        cols = slice(k * lanes, (k + 1) * lanes)
        head[:, cols] = grads[strided(k, pad), :]
        for row in range(2):
            sums[row : row + 1, cols] = (
                jnp.sum(total[row * groups + k], axis=0, keepdims=True) * scale
            )


def taps_kernel(grads, gated, sums, small, spread, *, taps, pad, seg, scale):
    groups = small.shape[1] // lanes
    unit = 4

    def tap_block(i, carry):
        base = i * unit
        carry = list(carry)
        grad = [grads[tile(base + u), :] for u in range(unit)]
        for m in range(unit + taps - 1):
            row = gated[tile(base + (pad - taps + 1) + m), :]
            for u in range(unit):
                j = m - u
                if 0 <= j < taps:
                    carry[j] = carry[j] + grad[u] * row
        return tuple(carry)

    zero = jnp.zeros((sublanes, lanes), jnp.float32)
    total = lax.fori_loop(0, seg // unit, tap_block, (zero,) * taps)
    for j in range(taps):
        spread[tile(j), :] = total[j] * scale
    small[...] = jnp.zeros_like(small)
    for k in range(groups):
        cols = slice(k * lanes, (k + 1) * lanes)
        small[:taps, cols] = sum(
            spread[strided(b, taps), :] for b in range(k, sublanes, groups)
        )
        small[taps : taps + 2, cols] = sums[:, cols]


def input_kernel(grads, halo, weight, value, gate, grad_value, grad_gate, taps_in, tail, conv, *, taps, pad, seg):
    length, channels = value.shape
    groups = channels // lanes
    segments = length // seg
    for k in range(groups):
        cols = slice(k * lanes, (k + 1) * lanes)
        for s in range(segments):
            b = s * groups + k
            taps_in[strided(b, taps), :] = weight[:, cols]
            after = grads[strided(b + groups, pad), :] if s + 1 < segments else halo[:, cols]
            tail[strided(pad * sublanes + b, pad), :] = after
    tail[: pad * sublanes, :] = grads[(seg - pad) * sublanes :, :]
    tap = [taps_in[tile(j), :] for j in range(taps)]
    unit = 16

    def block_of(source, offset):
        def conv_block(i, carry):
            base = i * unit
            sums = [None] * unit
            for m in range(unit + taps - 1):
                row = source[tile(base + m), :]
                for u in range(unit):
                    j = taps - 1 - (m - u)
                    if 0 <= j < taps:
                        term = tap[j] * row
                        sums[u] = term if sums[u] is None else sums[u] + term
            for u in range(unit):
                conv[tile(offset + base + u), :] = sums[u]
            return carry

        return conv_block

    lax.fori_loop(0, (seg - pad) // unit, block_of(grads, 0), 0)
    lax.fori_loop(0, pad // unit, block_of(tail, seg - pad), 0)
    chunk = 128
    for s in range(segments):

        def out_block(i, carry, s=s):
            base = pl.multiple_of(i * chunk, chunk)
            at = pl.multiple_of(s * seg + i * chunk, chunk)
            for k in range(groups):
                cols = slice(k * lanes, (k + 1) * lanes)
                grad = conv[strided(base * sublanes + s * groups + k, chunk), :]
                sig = jax.nn.sigmoid(gate[pl.ds(at, chunk), cols].astype(jnp.float32))
                by_value = grad * sig
                grad_value[pl.ds(at, chunk), cols] = by_value.astype(jnp.bfloat16)
                grad_gate[pl.ds(at, chunk), cols] = (
                    by_value * value[pl.ds(at, chunk), cols].astype(jnp.float32) * (1.0 - sig)
                ).astype(jnp.bfloat16)
            return carry

        lax.fori_loop(0, seg // chunk, out_block, 0)


def in_vmem(count):
    return [pl.BlockSpec(memory_space=pltpu.VMEM)] * count


def f32(*shape):
    return jax.ShapeDtypeStruct(shape, jnp.float32)


def small_part(small, count_dp):
    if count_dp == 1:
        return small
    half = small.shape[0] // 2
    index = lax.axis_index("dp") % 2
    other = exchange(lax.dynamic_slice_in_dim(small, (1 - index) * half, half, 0), lambda d: (0, 1))
    return lax.dynamic_slice_in_dim(small, index * half, half, 0) + other


def small_whole(mine, count_dp):
    for bit in bits_of(count_dp)[1:]:
        mine = mine + exchange(mine, lambda d, bit=bit: (0, bit))
    if count_dp == 1:
        return mine
    other = exchange(mine, lambda d: (0, 1))
    first = lax.axis_index("dp") % 2 == 0
    return jnp.where(
        first, jnp.concatenate([mine, other], axis=0), jnp.concatenate([other, mine], axis=0)
    )


def bits_of(count):
    return [1 << b for b in range(count.bit_length() - 1)]


def per_device(glu_value, glu_gate, cotangent, conv_weight, norm_gain, norm_shift, out_weight):
    value_rows = glu_value[0]
    gate_rows = glu_gate[0]
    cotan_rows = cotangent[0]
    length, channels = value_rows.shape
    taps = conv_weight.shape[0]
    features = out_weight.shape[0]
    count_sp = lax.axis_size("sp")
    count_dp = lax.axis_size("dp")
    scale = 1.0 / math.sqrt(length * count_sp * count_dp)
    pad = rounded_up(taps, 16)
    seg = length * (channels // lanes) // sublanes
    gain = norm_gain[None]
    shift = norm_shift[None]
    blocks = length // seg * (channels // lanes)

    weights = [out_weight] + [
        exchange(out_weight, lambda d, k=k: (0, k)) for k in range(1, count_dp)
    ]
    halo = lax.ppermute(
        jnp.concatenate([value_rows[length - pad :], gate_rows[length - pad :]], axis=0),
        "sp",
        [(i, i + 1) for i in range(count_sp - 1)],
    )
    others = count_dp - 1
    *sent, act, gated, normed, inv = pl.pallas_call(
        functools.partial(
            fwd_kernel, taps=taps, pad=pad, seg=seg, eps=epsilon, scale=scale, others=others
        ),
        out_shape=[f32(features, channels)] * others
        + [
            jax.ShapeDtypeStruct((length, channels), jnp.bfloat16),
            f32((pad + seg) * sublanes, lanes),
            f32(length, channels),
            f32(length, lanes),
        ],
        in_specs=in_vmem(7),
        out_specs=in_vmem(others + 4),
        scratch_shapes=[
            pltpu.VMEM((pad * sublanes, lanes), jnp.float32),
            pltpu.VMEM((seg * sublanes, lanes), jnp.float32),
        ],
        name="forward",
    )(value_rows, gate_rows, halo, cotan_rows, conv_weight, gain, shift)
    arrived = [exchange(sent[k - 1], lambda d, k=k: (0, k)) for k in range(1, count_dp)]

    own, grads, head, sums = pl.pallas_call(
        functools.partial(bwd_kernel, seg=seg, scale=scale, pieces=count_dp),
        out_shape=[
            f32(features, channels),
            f32(seg * sublanes, lanes),
            f32(pad, channels),
            f32(2, channels),
        ],
        in_specs=in_vmem(6 + count_dp),
        out_specs=in_vmem(4),
        scratch_shapes=[pltpu.VMEM((length, channels), jnp.float32)],
        name="backward",
    )(cotan_rows, act, normed, inv, gain, shift, *weights)
    later = lax.ppermute(head, "sp", [(i, i - 1) for i in range(1, count_sp)])
    small = pl.pallas_call(
        functools.partial(taps_kernel, taps=taps, pad=pad, seg=seg, scale=scale),
        out_shape=f32(rounded_up(taps + 2, 8), channels),
        in_specs=in_vmem(3),
        out_specs=in_vmem(1)[0],
        scratch_shapes=[pltpu.VMEM((pad * sublanes, lanes), jnp.float32)],
        name="taps",
    )(grads, gated, sums)
    grad_value, grad_gate = pl.pallas_call(
        functools.partial(input_kernel, taps=taps, pad=pad, seg=seg),
        out_shape=[jax.ShapeDtypeStruct((length, channels), jnp.bfloat16)] * 2,
        in_specs=in_vmem(5),
        out_specs=in_vmem(2),
        scratch_shapes=[
            pltpu.VMEM((pad * sublanes, lanes), jnp.float32),
            pltpu.VMEM((2 * pad * sublanes, lanes), jnp.float32),
            pltpu.VMEM((seg * sublanes, lanes), jnp.float32),
        ],
        name="inputs",
    )(grads, later, conv_weight, value_rows, gate_rows)

    steps = len(levels_of(count_sp, 0))
    rows = tree([own] + arrived)
    for step in range(steps):
        rows = reduce_level(rows, step, jnp.bfloat16 if step == 0 else jnp.float32)
    rows = rows.astype(jnp.bfloat16)
    mine = small_part(small, count_dp)
    for step in reversed(range(steps)):
        rows, mine = gather_level(rows, mine, step)
    grad_out_weight = rows.astype(jnp.float32)
    small = small_whole(mine, count_dp)
    return (
        grad_value[None],
        grad_gate[None],
        grad_out_weight,
        small[:taps],
        small[taps],
        small[taps + 1],
    )


def solution(mesh):
    in_specs = (
        P("dp", "sp", None),
        P("dp", "sp", None),
        P("dp", "sp", None),
        P(),
        P(),
        P(),
        P("dp", None),
    )
    out_specs = (P("dp", "sp", None), P("dp", "sp", None), P("dp", None), P(), P(), P())
    return jax.shard_map(
        per_device, mesh=mesh, in_specs=in_specs, out_specs=out_specs, check_vma=False
    )
```

time: 132 us -> 89.4 us (0.68)
  starting transfers between devices: 48.6 us -> 25.8 us
  waiting for transfers between devices: 36.5 us -> 24.7 us
  Pallas kernels: 34.7 us -> 25.7 us
    ppermute x33 -> x16, starting transfers between devices: 42.5 us -> 19.6 us  [exchange(): return lax.ppermute(value, ('sp', 'dp'), pairs)]
    ppermute x33 -> x16, waiting for transfers between devices: 29.9 us -> 15.9 us  [exchange(): return lax.ppermute(value, ('sp', 'dp'), pairs)]
    pallas_call x1, Pallas kernels: 12.2 us -> 8.13 us  [per_device(): pl.pallas_call(functools.partial(fwd_kernel, taps=taps, pad=pad, seg=seg,...]
    pallas_call x1, Pallas kernels: 8.17 us -> 5.01 us  [per_device(): pl.pallas_call(functools.partial(taps_kernel, taps=taps, pad=pad, seg=seg...]
    ppermute x1, waiting for transfers between devices: 4.69 us -> 6.91 us  [per_device(): later = lax.ppermute(head, 'sp', [(i, i - 1) for i in range(1, count_sp)])]
    pallas_call x1, Pallas kernels: 7.55 us -> 5.4 us  [per_device(): pl.pallas_call(functools.partial(input_kernel, taps=taps, pad=pad, seg=se...]
    add x4 -> x2, other arithmetic: 3.02 us -> 2.74 us  [tree(): items = [items[i] + items[i + 1] for i in range(0, len(items), 2)]]
  transfers between devices with their start and end apart: 35 -> 18, of which waited for: 16 -> 7; matrix products, arithmetic and copies ran while one was open for 4% -> 5% of each run, Pallas kernels for 17% -> 20%
where the time goes in v3:
time: 89.4 us; the launch traced here: 89.1 us
  starting transfers between devices  25.8 us (29%)
  Pallas kernels  25.7 us (29%)
  waiting for transfers between devices  24.7 us (28%)
  other arithmetic  6.19 us (7%)
  local copies, waits for them, and re-layouts  5.78 us (6%)
  between operations  0.92 us (1%)
    ppermute x16, starting transfers between devices, exchange(): return lax.ppermute(value, ('sp', 'dp'), pairs)  19.6 us
    ppermute x16, waiting for transfers between devices, exchange(): return lax.ppermute(value, ('sp', 'dp'), pairs)  15.9 us
    pallas_call x1, Pallas kernels, per_device(): pl.pallas_call(functools.partial(fwd_kernel, taps=taps, pad=pad, seg=seg,...  8.13 us
    pallas_call x1, Pallas kernels, per_device(): pl.pallas_call(functools.partial(bwd_kernel, seg=seg, scale=scale, pieces...  7.14 us
    ppermute x1, waiting for transfers between devices, per_device(): later = lax.ppermute(head, 'sp', [(i, i - 1) for i in range(1, count_sp)])  6.91 us
    pallas_call x1, Pallas kernels, per_device(): pl.pallas_call(functools.partial(input_kernel, taps=taps, pad=pad, seg=se...  5.4 us
    pallas_call x1, Pallas kernels, per_device(): pl.pallas_call(functools.partial(taps_kernel, taps=taps, pad=pad, seg=seg...  5.01 us
    ppermute x1, starting transfers between devices, per_device(): lax.ppermute(jnp.concatenate([value_rows[length - pad:], gate_rows[length...  4.87 us
  transfers between devices with their start and end apart: 18, of which 7 were waited for; matrix products, arithmetic and copies ran while one was open for 5% of the time, Pallas kernels for 20%

profile of v3, /device:TPU:0, one launch (start us, length us, event | category | flops | bytes accessed | tf_op | source)
XLA Modules:
  0.0 89.1 jit_solution(18183095929285959824)
XLA Ops:
  0.6 0.0 copy-start.1
  0.6 0.9 slice_bitcast_fusion
  1.5 4.9 %collective-permute-start = (bf16[64,512]{1,0:T(8,128)(2,1)S(1)}, bf16[64,512]{1,0:T(8,128)(2,1)S(1)}, u32[]{:S(2)}, u32[]{:S(2)}) collective-permute-start(bf16[64,512]{1,0:T(8,128)(2,1)S(1)} %pad_maximum_fusion.2), channel_id=1, source_target_pairs={{0,2},{2,4},{4,6},{6,8},{8,10},{10,12},{12,14},{14,16},{16,18},{18... | collective-permute-start | bytes 196616 | tf_op jit(solution)/shard_map/ppermute | solution.py:397
  6.4 1.9 %collective-permute-done.halo = bf16[64,512]{1,0:T(8,128)(2,1)S(1)} collective-permute-done((bf16[64,512]{1,0:T(8,128)(2,1)S(1)}, bf16[64,512]{1,0:T(8,128)(2,1)S(1)}, u32[]{:S(2)}, u32[]{:S(2)}) %collective-permute-start) | collective-permute-done | bytes 65568 | tf_op jit(solution)/shard_map/ppermute | solution.py:397
  8.3 0.6 copy-done.4
  8.9 8.1 %forward.1 = (f32[1024,512]{1,0:T(8,128)}, bf16[512,512]{1,0:T(8,128)(2,1)}, f32[2304,128]{1,0:T(8,128)}, f32[512,512]{1,0:T(8,128)}, f32[512,128]{1,0:T(8,128)}) custom-call(bf16[512,512]{1,0:T(8,128)(2,1)} %bitcast.15, bf16[512,512]{1,0:T(8,128)(2,1)} %bitcast.17, bf16[64,512]{1,0:T(8,128)(2,1)} %copy-done.4, bf16[512,2048]{1,0:T(8,128)(2,1)} %bitcast.13, ...), custom_call_target="tpu_custom_call" | custom-call | tf_op jit(solution)/shard_map/forward/pallas_call | solution.py:403
  17.1 0.5 collective-permute-start.1
  17.6 5.5 %collective-permute-done.1.rest_1_ = bf16[1024,512]{1,0:T(8,128)(2,1)} collective-permute-done((bf16[1024,512]{1,0:T(8,128)(2,1)S(1)}, bf16[1024,512]{1,0:T(8,128)(2,1)}, u32[]{:S(2)}, u32[]{:S(2)}) %collective-permute-start.1) | collective-permute-done | bytes 1048608 | tf_op jit(solution)/shard_map/ppermute | solution.py:22
  23.1 7.1 %backward.1 = (f32[1024,512]{1,0:T(8,128)}, f32[2048,128]{1,0:T(8,128)}, f32[32,512]{1,0:T(8,128)}, f32[2,512]{1,0:T(2,128)}) custom-call(bf16[512,2048]{1,0:T(8,128)(2,1)} %bitcast.14, bf16[512,512]{1,0:T(8,128)(2,1)} %get-tuple-element.17.act, f32[512,512]{1,0:T(8,128)} %get-tuple-element.18.normed, f32[512,128]{1,0:T(8,128)} %get-tuple-element.19.inv_in, ...), custom_call_target="tpu_custom_call" | custom-call | tf_op jit(solution)/shard_map/backward/pallas_call | solution.py:424
  30.2 1.3 %copy-done = f32[1024,512]{1,0:T(8,128)} copy-done((f32[1024,512]{1,0:T(8,128)}, f32[1024,512]{1,0:T(8,128)S(1)}, u32[]{:S(2)}) %copy-start) | copy-done | bytes 2097176
  31.5 2.7 %add.133 = f32[1024,512]{1,0:T(8,128)S(1)} add(f32[1024,512]{1,0:T(8,128)} %get-tuple-element.24, f32[1024,512]{1,0:T(8,128)} %copy-done) | non-fusion elementwise | flops 524288 | bytes 6291456 | tf_op jit(solution)/shard_map/add | solution.py:71
  34.2 0.1 dynamic-slice_convert_fusion.2
  34.3 3.4 %collective-permute-start.4 = (bf16[256,512]{1,0:T(8,128)(2,1)S(1)}, bf16[256,512]{1,0:T(8,128)(2,1)S(1)}, u32[]{:S(2)}, u32[]{:S(2)}) collective-permute-start(bf16[256,512]{1,0:T(8,128)(2,1)S(1)} %get-tuple-element.32), channel_id=1, source_target_pairs={{0,6},{2,4},{4,2},{6,0},{8,14},{10,12},{12,10},{14,8},{16,22},{18,... | collective-permute-start | bytes 786440 | tf_op jit(solution)/shard_map/ppermute | solution.py:22
  37.7 0.5 collective-permute-start.5
  38.2 0.9 %collective-permute-start.6 = (bf16[256,512]{1,0:T(8,128)(2,1)S(1)}, bf16[256,512]{1,0:T(8,128)(2,1)}, u32[]{:S(2)}, u32[]{:S(2)}) collective-permute-start(bf16[256,512]{1,0:T(8,128)(2,1)S(1)} %get-tuple-element.33), channel_id=1, source_target_pairs={{0,2},{2,0},{4,6},{6,4},{8,10},{10,8},{12,14},{14,12},{16,18},{18,... | collective-permute-start | bytes 786440 | tf_op jit(solution)/shard_map/ppermute | solution.py:22
  39.2 5.0 %taps.1 = f32[40,512]{1,0:T(8,128)} custom-call(f32[2048,128]{1,0:T(8,128)} %get-tuple-element.20.grads, f32[2304,128]{1,0:T(8,128)} %get-tuple-element.26.gated, f32[2,512]{1,0:T(2,128)} %get-tuple-element.27.sums), custom_call_target="tpu_custom_call" | custom-call | tf_op jit(solution)/shard_map/taps/pallas_call | solution.py:438
  44.2 0.9 constant_dynamic-slice_fusion
  45.1 1.8 %collective-permute-start.10 = (f32[20,512]{1,0:T(8,128)S(1)}, f32[20,512]{1,0:T(8,128)S(1)}, u32[]{:S(2)}, u32[]{:S(2)}) collective-permute-start(f32[20,512]{1,0:T(8,128)S(1)} %constant_dynamic-slice_fusion), channel_id=1, source_target_pairs={{0,1},{2,3},{4,5},{6,7},{8,9},{10,11},{12,13},{14,15},{16,17},{18,... | collective-permute-start | bytes 122888 | tf_op jit(solution)/shard_map/ppermute | solution.py:22
  46.8 0.0 collective-permute-done.4
  46.8 0.0 collective-permute-done.5
  46.8 0.0 collective-permute-done.6
  46.8 1.1 %convert_add_fusion = f32[256,512]{1,0:T(8,128)S(1)} fusion(bf16[256,512]{1,0:T(8,128)(2,1)} %collective-permute-done.6, bf16[256,512]{1,0:T(8,128)(2,1)S(1)} %collective-permute-done.5, bf16[256,512]{1,0:T(8,128)(2,1)S(1)} %collective-permute-done.4, f32[1024,512]{1,0:T(8,128)S(1)} %add.133, s32[]{:T(128)S(6)} %select_n.165), kind=kLoop, calls=%fused_computation.4 | loop fusion | flops 786432 | bytes 1835012 | tf_op jit(solution)/shard_map/add | solution.py:65
  47.9 0.0 copy-start.5
  48.0 3.7 %collective-permute-start.7 = (f32[64,512]{1,0:T(8,128)S(1)}, f32[64,512]{1,0:T(8,128)S(1)}, u32[]{:S(2)}, u32[]{:S(2)}) collective-permute-start(f32[64,512]{1,0:T(8,128)S(1)} %get-tuple-element.35), channel_id=1, source_target_pairs={{0,24},{2,26},{4,28},{6,30},{8,16},{10,18},{12,20},{14,22},{16,8},... | collective-permute-start | bytes 393224 | tf_op jit(solution)/shard_map/ppermute | solution.py:22
  51.7 0.0 collective-permute-start.8
  51.7 0.7 collective-permute-start.9
  52.4 0.0 collective-permute-done.10
  52.5 2.5 %collective-permute-done.7 = f32[64,512]{1,0:T(8,128)S(1)} collective-permute-done((f32[64,512]{1,0:T(8,128)S(1)}, f32[64,512]{1,0:T(8,128)S(1)}, u32[]{:S(2)}, u32[]{:S(2)}) %collective-permute-start.7) | collective-permute-done | bytes 131104 | tf_op jit(solution)/shard_map/ppermute | solution.py:22
  54.9 3.4 %collective-permute-done.8 = f32[64,512]{1,0:T(8,128)S(1)} collective-permute-done((f32[64,512]{1,0:T(8,128)S(1)}, f32[64,512]{1,0:T(8,128)S(1)}, u32[]{:S(2)}, u32[]{:S(2)}) %collective-permute-start.8) | collective-permute-done | bytes 131104 | tf_op jit(solution)/shard_map/ppermute | solution.py:22
  58.4 2.5 %collective-permute-start.11 = (bf16[104,512]{1,0:T(8,128)(2,1)S(1)}, bf16[104,512]{1,0:T(8,128)(2,1)S(1)}, u32[]{:S(2)}, u32[]{:S(2)}) collective-permute-start(bf16[104,512]{1,0:T(8,128)(2,1)S(1)} %pad_maximum_fusion.1), channel_id=1, source_target_pairs={{0,24},{2,26},{4,28},{6,30},{8,16},{10,18},{12,20},{14,22},{16,8},... | collective-permute-start | bytes 319496 | tf_op jit(solution)/shard_map/ppermute | solution.py:22
  60.9 0.2 collective-permute-start.12
  61.1 1.7 %collective-permute-start.13 = (bf16[104,512]{1,0:T(8,128)(2,1)S(1)}, bf16[104,512]{1,0:T(8,128)(2,1)S(1)}, u32[]{:S(2)}, u32[]{:S(2)}) collective-permute-start(bf16[104,512]{1,0:T(8,128)(2,1)S(1)} %pad_maximum_fusion.1), channel_id=1, source_target_pairs={{0,8},{2,10},{4,12},{6,14},{8,0},{10,2},{12,4},{14,6},{16,24},{18,... | collective-permute-start | bytes 319496 | tf_op jit(solution)/shard_map/ppermute | solution.py:22
  62.8 2.1 %collective-permute-done.11 = bf16[104,512]{1,0:T(8,128)(2,1)S(1)} collective-permute-done((bf16[104,512]{1,0:T(8,128)(2,1)S(1)}, bf16[104,512]{1,0:T(8,128)(2,1)S(1)}, u32[]{:S(2)}, u32[]{:S(2)}) %collective-permute-start.11) | collective-permute-done | bytes 106528 | tf_op jit(solution)/shard_map/ppermute | solution.py:22
  65.0 2.4 %collective-permute-done.12 = bf16[104,512]{1,0:T(8,128)(2,1)S(1)} collective-permute-done((bf16[104,512]{1,0:T(8,128)(2,1)S(1)}, bf16[104,512]{1,0:T(8,128)(2,1)S(1)}, u32[]{:S(2)}, u32[]{:S(2)}) %collective-permute-start.12) | collective-permute-done | bytes 106528 | tf_op jit(solution)/shard_map/ppermute | solution.py:22
  67.6 0.1 maximum_select_fusion.3
  67.7 0.8 collective-permute-start.14
  68.5 0.7 collective-permute-start.15
  69.2 2.1 %collective-permute-start.16 = (bf16[296,512]{1,0:T(8,128)(2,1)S(1)}, bf16[296,512]{1,0:T(8,128)(2,1)S(1)}, u32[]{:S(2)}, u32[]{:S(2)}) collective-permute-start(bf16[296,512]{1,0:T(8,128)(2,1)S(1)} %pad_maximum_fusion), channel_id=1, source_target_pairs={{0,2},{2,0},{4,6},{6,4},{8,10},{10,8},{12,14},{14,12},{16,18},{18,... | collective-permute-start | bytes 909320 | tf_op jit(solution)/shard_map/ppermute | solution.py:22
  71.2 1.3 %collective-permute-start.2 = (f32[32,512]{1,0:T(8,128)S(1)}, f32[32,512]{1,0:T(8,128)S(1)}, u32[]{:S(2)}, u32[]{:S(2)}) collective-permute-start(f32[32,512]{1,0:T(8,128)S(1)} %copy-done.5), channel_id=1, source_target_pairs={{2,0},{4,2},{6,4},{8,6},{10,8},{12,10},{14,12},{16,14},{18,16},{20... | collective-permute-start | bytes 196616 | tf_op jit(solution)/shard_map/ppermute | solution.py:437
  72.6 6.9 %collective-permute-done.2.halo = f32[32,512]{1,0:T(8,128)S(1)} collective-permute-done((f32[32,512]{1,0:T(8,128)S(1)}, f32[32,512]{1,0:T(8,128)S(1)}, u32[]{:S(2)}, u32[]{:S(2)}) %collective-permute-start.2) | collective-permute-done | bytes 65568 | tf_op jit(solution)/shard_map/ppermute | solution.py:437
  79.5 0.6 copy-done.3
  80.1 5.4 %inputs.1 = (bf16[512,512]{1,0:T(8,128)(2,1)}, bf16[512,512]{1,0:T(8,128)(2,1)}) custom-call(f32[2048,128]{1,0:T(8,128)} %get-tuple-element.20.grads, f32[32,512]{1,0:T(8,128)} %copy-done.3, f32[31,512]{1,0:T(8,128)} %weight.3, bf16[512,512]{1,0:T(8,128)(2,1)} %bitcast.16, bf16[512,512]{1,0:T(8,128)(2,1)} %bitcast.18), custom_call_target="tpu_custom_call" | custom-call | tf_op jit(solution)/shard_map/inputs/pallas_call | solution.py:446
  85.6 0.1 collective-permute-start.17
  85.7 0.2 maximum_select_fusion.2
  86.0 0.2 maximum_select_fusion.1
  86.2 1.7 %fusion = f32[1024,512]{1,0:T(8,128)} fusion(bf16[512,512]{1,0:T(8,128)(2,1)S(1)} %maximum_select_fusion.2, bf16[512,512]{1,0:T(8,128)(2,1)S(1)} %maximum_select_fusion.1, pred[]{:T(512)S(6)} %eq.39), kind=kLoop, calls=%fused_computation.1 | loop fusion | flops 5242880 | bytes 3145729 | tf_op jit(solution)/shard_map/convert_element_type | solution.py:467
  87.9 0.6 slice.118
  88.5 0.6 fusion.11
  (33 shorter events, 0.4 us)
Async XLA Ops:
  0.6 16.4 %copy-start.1 = (bf16[1024,512]{1,0:T(8,128)(2,1)S(1)}, bf16[1024,512]{1,0:T(8,128)(2,1)}, u32[]{:S(2)}) copy-start(bf16[1024,512]{1,0:T(8,128)(2,1)} %rest_0_.1) | copy-start | bytes 3145732
  1.5 6.8 %collective-permute-start = (bf16[64,512]{1,0:T(8,128)(2,1)S(1)}, bf16[64,512]{1,0:T(8,128)(2,1)S(1)}, u32[]{:S(2)}, u32[]{:S(2)}) collective-permute-start(bf16[64,512]{1,0:T(8,128)(2,1)S(1)} %pad_maximum_fusion.2), channel_id=1, source_target_pairs={{0,2},{2,4},{4,6},{6,8},{8,10},{10,12},{12,14},{14,16},{16,18},{18... | collective-permute-start | bytes 196616 | tf_op jit(solution)/shard_map/ppermute | solution.py:397
  8.3 0.6 copy-start.4
  17.0 13.1 %collective-permute-start.3 = (f32[1024,512]{1,0:T(8,128)}, f32[1024,512]{1,0:T(8,128)S(1)}, u32[]{:S(2)}, u32[]{:S(2)}) collective-permute-start(f32[1024,512]{1,0:T(8,128)} %get-tuple-element.25), channel_id=1, source_target_pairs={{0,1},{2,3},{4,5},{6,7},{8,9},{10,11},{12,13},{14,15},{16,17},{18,... | collective-permute-start | bytes 6291464 | tf_op jit(solution)/shard_map/ppermute | solution.py:22
  17.1 6.0 %collective-permute-start.1 = (bf16[1024,512]{1,0:T(8,128)(2,1)S(1)}, bf16[1024,512]{1,0:T(8,128)(2,1)}, u32[]{:S(2)}, u32[]{:S(2)}) collective-permute-start(bf16[1024,512]{1,0:T(8,128)(2,1)S(1)} %copy-done.1), channel_id=1, source_target_pairs={{0,1},{2,3},{4,5},{6,7},{8,9},{10,11},{12,13},{14,15},{16,17},{18,... | collective-permute-start | bytes 3145736 | tf_op jit(solution)/shard_map/ppermute | solution.py:22
  30.2 1.3 %copy-start = (f32[1024,512]{1,0:T(8,128)}, f32[1024,512]{1,0:T(8,128)S(1)}, u32[]{:S(2)}) copy-start(f32[1024,512]{1,0:T(8,128)S(1)} %collective-permute-done.3) | copy-start | bytes 6291460
  34.3 12.5 %collective-permute-start.4 = (bf16[256,512]{1,0:T(8,128)(2,1)S(1)}, bf16[256,512]{1,0:T(8,128)(2,1)S(1)}, u32[]{:S(2)}, u32[]{:S(2)}) collective-permute-start(bf16[256,512]{1,0:T(8,128)(2,1)S(1)} %get-tuple-element.32), channel_id=1, source_target_pairs={{0,6},{2,4},{4,2},{6,0},{8,14},{10,12},{12,10},{14,8},{16,22},{18,... | collective-permute-start | bytes 786440 | tf_op jit(solution)/shard_map/ppermute | solution.py:22
  37.7 9.1 %collective-permute-start.5 = (bf16[256,512]{1,0:T(8,128)(2,1)S(1)}, bf16[256,512]{1,0:T(8,128)(2,1)S(1)}, u32[]{:S(2)}, u32[]{:S(2)}) collective-permute-start(bf16[256,512]{1,0:T(8,128)(2,1)S(1)} %get-tuple-element.34), channel_id=1, source_target_pairs={{0,4},{2,6},{4,0},{6,2},{8,12},{10,14},{12,8},{14,10},{16,20},{18,... | collective-permute-start | bytes 786440 | tf_op jit(solution)/shard_map/ppermute | solution.py:22
  38.2 8.6 %collective-permute-start.6 = (bf16[256,512]{1,0:T(8,128)(2,1)S(1)}, bf16[256,512]{1,0:T(8,128)(2,1)}, u32[]{:S(2)}, u32[]{:S(2)}) collective-permute-start(bf16[256,512]{1,0:T(8,128)(2,1)S(1)} %get-tuple-element.33), channel_id=1, source_target_pairs={{0,2},{2,0},{4,6},{6,4},{8,10},{10,8},{12,14},{14,12},{16,18},{18,... | collective-permute-start | bytes 786440 | tf_op jit(solution)/shard_map/ppermute | solution.py:22
  44.2 8.3 %copy-start.2 = (f32[40,512]{1,0:T(8,128)S(1)}, f32[40,512]{1,0:T(8,128)}, u32[]{:S(2)}) copy-start(f32[40,512]{1,0:T(8,128)} %taps.1) | copy-start | bytes 245764
  45.1 7.4 %collective-permute-start.10 = (f32[20,512]{1,0:T(8,128)S(1)}, f32[20,512]{1,0:T(8,128)S(1)}, u32[]{:S(2)}, u32[]{:S(2)}) collective-permute-start(f32[20,512]{1,0:T(8,128)S(1)} %constant_dynamic-slice_fusion), channel_id=1, source_target_pairs={{0,1},{2,3},{4,5},{6,7},{8,9},{10,11},{12,13},{14,15},{16,17},{18,... | collective-permute-start | bytes 122888 | tf_op jit(solution)/shard_map/ppermute | solution.py:22
  47.9 23.3 %copy-start.5 = (f32[32,512]{1,0:T(8,128)S(1)}, f32[32,512]{1,0:T(8,128)}, u32[]{:S(2)}) copy-start(f32[32,512]{1,0:T(8,128)} %get-tuple-element.21) | copy-start | bytes 196612
  48.0 6.9 %collective-permute-start.7 = (f32[64,512]{1,0:T(8,128)S(1)}, f32[64,512]{1,0:T(8,128)S(1)}, u32[]{:S(2)}, u32[]{:S(2)}) collective-permute-start(f32[64,512]{1,0:T(8,128)S(1)} %get-tuple-element.35), channel_id=1, source_target_pairs={{0,24},{2,26},{4,28},{6,30},{8,16},{10,18},{12,20},{14,22},{16,8},... | collective-permute-start | bytes 393224 | tf_op jit(solution)/shard_map/ppermute | solution.py:22
  51.7 6.6 %collective-permute-start.8 = (f32[64,512]{1,0:T(8,128)S(1)}, f32[64,512]{1,0:T(8,128)S(1)}, u32[]{:S(2)}, u32[]{:S(2)}) collective-permute-start(f32[64,512]{1,0:T(8,128)S(1)} %get-tuple-element.37), channel_id=1, source_target_pairs={{0,16},{2,18},{4,20},{6,22},{8,24},{10,26},{12,28},{14,30},{16,0},... | collective-permute-start | bytes 393224 | tf_op jit(solution)/shard_map/ppermute | solution.py:22
  51.7 6.6 %collective-permute-start.9 = (f32[64,512]{1,0:T(8,128)S(1)}, f32[64,512]{1,0:T(8,128)S(1)}, u32[]{:S(2)}, u32[]{:S(2)}) collective-permute-start(f32[64,512]{1,0:T(8,128)S(1)} %get-tuple-element.36), channel_id=1, source_target_pairs={{0,8},{2,10},{4,12},{6,14},{8,0},{10,2},{12,4},{14,6},{16,24},{18,... | collective-permute-start | bytes 393224 | tf_op jit(solution)/shard_map/ppermute | solution.py:22
  58.4 6.6 %collective-permute-start.11 = (bf16[104,512]{1,0:T(8,128)(2,1)S(1)}, bf16[104,512]{1,0:T(8,128)(2,1)S(1)}, u32[]{:S(2)}, u32[]{:S(2)}) collective-permute-start(bf16[104,512]{1,0:T(8,128)(2,1)S(1)} %pad_maximum_fusion.1), channel_id=1, source_target_pairs={{0,24},{2,26},{4,28},{6,30},{8,16},{10,18},{12,20},{14,22},{16,8},... | collective-permute-start | bytes 319496 | tf_op jit(solution)/shard_map/ppermute | solution.py:22
  60.9 6.5 %collective-permute-start.12 = (bf16[104,512]{1,0:T(8,128)(2,1)S(1)}, bf16[104,512]{1,0:T(8,128)(2,1)S(1)}, u32[]{:S(2)}, u32[]{:S(2)}) collective-permute-start(bf16[104,512]{1,0:T(8,128)(2,1)S(1)} %pad_maximum_fusion.1), channel_id=1, source_target_pairs={{0,16},{2,18},{4,20},{6,22},{8,24},{10,26},{12,28},{14,30},{16,0},... | collective-permute-start | bytes 319496 | tf_op jit(solution)/shard_map/ppermute | solution.py:22
  61.1 6.3 %collective-permute-start.13 = (bf16[104,512]{1,0:T(8,128)(2,1)S(1)}, bf16[104,512]{1,0:T(8,128)(2,1)S(1)}, u32[]{:S(2)}, u32[]{:S(2)}) collective-permute-start(bf16[104,512]{1,0:T(8,128)(2,1)S(1)} %pad_maximum_fusion.1), channel_id=1, source_target_pairs={{0,8},{2,10},{4,12},{6,14},{8,0},{10,2},{12,4},{14,6},{16,24},{18,... | collective-permute-start | bytes 319496 | tf_op jit(solution)/shard_map/ppermute | solution.py:22
  67.7 17.8 %collective-permute-start.14 = (bf16[296,512]{1,0:T(8,128)(2,1)S(1)}, bf16[296,512]{1,0:T(8,128)(2,1)S(1)}, u32[]{:S(2)}, u32[]{:S(2)}) collective-permute-start(bf16[296,512]{1,0:T(8,128)(2,1)S(1)} %pad_maximum_fusion), channel_id=1, source_target_pairs={{0,6},{2,4},{4,2},{6,0},{8,14},{10,12},{12,10},{14,8},{16,22},{18,... | collective-permute-start | bytes 909320 | tf_op jit(solution)/shard_map/ppermute | solution.py:22
  68.5 17.1 %collective-permute-start.15 = (bf16[296,512]{1,0:T(8,128)(2,1)S(1)}, bf16[296,512]{1,0:T(8,128)(2,1)S(1)}, u32[]{:S(2)}, u32[]{:S(2)}) collective-permute-start(bf16[296,512]{1,0:T(8,128)(2,1)S(1)} %pad_maximum_fusion), channel_id=1, source_target_pairs={{0,4},{2,6},{4,0},{6,2},{8,12},{10,14},{12,8},{14,10},{16,20},{18,... | collective-permute-start | bytes 909320 | tf_op jit(solution)/shard_map/ppermute | solution.py:22
  69.2 16.4 %collective-permute-start.16 = (bf16[296,512]{1,0:T(8,128)(2,1)S(1)}, bf16[296,512]{1,0:T(8,128)(2,1)S(1)}, u32[]{:S(2)}, u32[]{:S(2)}) collective-permute-start(bf16[296,512]{1,0:T(8,128)(2,1)S(1)} %pad_maximum_fusion), channel_id=1, source_target_pairs={{0,2},{2,0},{4,6},{6,4},{8,10},{10,8},{12,14},{14,12},{16,18},{18,... | collective-permute-start | bytes 909320 | tf_op jit(solution)/shard_map/ppermute | solution.py:22
  71.2 8.3 %collective-permute-start.2 = (f32[32,512]{1,0:T(8,128)S(1)}, f32[32,512]{1,0:T(8,128)S(1)}, u32[]{:S(2)}, u32[]{:S(2)}) collective-permute-start(f32[32,512]{1,0:T(8,128)S(1)} %copy-done.5), channel_id=1, source_target_pairs={{2,0},{4,2},{6,4},{8,6},{10,8},{12,10},{14,12},{16,14},{18,16},{20... | collective-permute-start | bytes 196616 | tf_op jit(solution)/shard_map/ppermute | solution.py:437
  79.5 0.6 copy-start.3
  85.6 2.3 %collective-permute-start.17 = (f32[20,512]{1,0:T(8,128)S(1)}, f32[20,512]{1,0:T(8,128)S(1)}, u32[]{:S(2)}, u32[]{:S(2)}) collective-permute-start(f32[20,512]{1,0:T(8,128)S(1)} %fusion.6), channel_id=1, source_target_pairs={{0,1},{2,3},{4,5},{6,7},{8,9},{10,11},{12,13},{14,15},{16,17},{18,... | collective-permute-start | bytes 122888 | tf_op jit(solution)/shard_map/ppermute | solution.py:22
